TPU v7x, 32 devices: a whole 2x2x4 slice. The times are simulated.
32 devices in a mesh: ep: 8 (over z, x), tp: 4 (over y, core).
Axes of the slice: x: 2, y: 2, z: 4, core: 2. Of those that a mesh axis runs over, the one named last changes fastest.
Arguments:
- queries: bfloat16 [2048, 1024], P('ep', 'tp'), may hold values from -6 to 6
- keys: bfloat16 [2048, 256], P('ep', 'tp'), may hold values from -6 to 6
- values: bfloat16 [2048, 256], P('ep', 'tp'), may hold values from -6 to 6
- q_gain: float32 [64], replicated, may hold values from 1 to 6
- k_gain: float32 [64], replicated, may hold values from 1 to 6
- out_weight: bfloat16 [1024, 2048], P('tp'), may hold values from -0.1875 to 0.1875
- tokens: bfloat16 [1024, 2048], P(('ep', 'tp')), may hold values from -6 to 6
- ffn_gain: float32 [2048], replicated, may hold values from 0.1 to 1.9
- route: int32 [1024, 2], P(('ep', 'tp')), may hold values from 0 to 7, all different within a row; in each aligned block of 32 rows (0 to 31, 32 to 63, ...) at most 16 rows name the same one
- route_weight: float32 [1024, 2], P(('ep', 'tp')), may hold values from 0.1 to 1
- gate_weight: bfloat16 [8, 2048, 3584], P('ep', None, 'tp'), may hold values from -0.125 to 0.125
- up_weight: bfloat16 [8, 2048, 3584], P('ep', None, 'tp'), may hold values from -0.125 to 0.125
- down_weight: bfloat16 [8, 3584, 2048], P('ep', 'tp'), may hold values from -0.09375 to 0.09375
Outputs:
- mixer_out: bfloat16 [2048, 2048], P(('ep', 'tp'))
- mixed: bfloat16 [1024, 2048], P(('ep', 'tp'))
Inputs may be any that keep to these rules, and one draw needn't show every extreme that they name: `route`: each row names 2 different experts. In every device's aligned block of 32 rows no expert is named more than 16 times, and in some blocks some expert is named exactly 16 times.
All inputs are finite; a program needn't handle non-finite values.
Results may differ from a plain program's by a relative error of at most 0.013.
The roundings to bfloat16 on the way count: a program that leaves them out, or rounds other values in their place, can miss the bound.
Values may be sent and summed in bfloat16 or wider, within the bound.
No kernel may reach another device: no remote copies, remote signals or barrier semaphores. Data moves between devices by JAX's collectives and lax.ppermute only.
A program may use at most 192 MiB of HBM per device.

v0:
```python
import jax
import jax.numpy as jnp
from jax import lax
from jax.sharding import PartitionSpec as P

GRID_W = 64


EPS = 1e-06
THETA = 10000.0


def head_norm(vals, gain):
    vals = vals.astype(jnp.float32)
    return vals * lax.rsqrt(jnp.mean(vals * vals, axis=-1, keepdims=True) + EPS) * gain


def rotate(vals, positions):
    pairs = vals.shape[-1] // 2
    quarter = pairs // 2
    freqs = THETA ** (-jnp.arange(quarter, dtype=jnp.float32) / quarter)
    grid_row = (positions // GRID_W).astype(jnp.float32)
    grid_col = (positions % GRID_W).astype(jnp.float32)
    angle = jnp.concatenate([grid_row[:, None] * freqs, grid_col[:, None] * freqs], axis=-1)
    cosine = jnp.cos(angle)[:, None, :]
    sine = jnp.sin(angle)[:, None, :]
    split = vals.reshape(vals.shape[:-1] + (pairs, 2))
    first = split[..., 0]
    second = split[..., 1]
    turned = jnp.stack([first * cosine - second * sine, first * sine + second * cosine], axis=-1)
    return turned.reshape(vals.shape)


def local(
    queries,
    keys,
    values,
    q_gain,
    k_gain,
    out_weight,
    tokens,
    ffn_gain,
    route,
    route_weight,
    gate_weight,
    up_weight,
    down_weight,
):
    local_rows = queries.shape[0]
    head_size = q_gain.shape[0]
    query_heads = queries.shape[1] // head_size
    key_heads = keys.shape[1] // head_size
    group = query_heads // key_heads
    key_width = key_heads * head_size
    positions = lax.axis_index("ep") * local_rows + jnp.arange(local_rows, dtype=jnp.int32)
    rot_q = rotate(
        head_norm(queries.reshape(local_rows, query_heads, head_size), q_gain), positions
    ).astype(jnp.bfloat16)
    rot_q = rot_q.reshape(local_rows, key_heads, group, head_size)
    rot_k = rotate(
        head_norm(keys.reshape(local_rows, key_heads, head_size), k_gain), positions
    ).astype(jnp.bfloat16)
    joined = jnp.concatenate([rot_k.reshape(local_rows, key_width), values], axis=1)
    scale = head_size ** (-0.5)

    def fold_block(carry, block):
        highest, denom, numer = carry
        key_block = block[:, :key_width].reshape(-1, key_heads, head_size)
        value_block = block[:, key_width:].reshape(-1, key_heads, head_size)
        scores = (
            jnp.einsum("qkgd,skd->qkgs", rot_q, key_block, preferred_element_type=jnp.float32)
            * scale
        )
        new_high = jnp.maximum(highest, jnp.max(scores, axis=-1))
        shrink = jnp.exp(highest - new_high)
        expo = jnp.exp(scores - new_high[..., None])
        denom = denom * shrink + jnp.sum(expo, axis=-1)
        numer = numer * shrink[..., None] + jnp.einsum(
            "qkgs,skd->qkgd",
            expo.astype(jnp.bfloat16),
            value_block,
            preferred_element_type=jnp.float32,
        )
        return ((new_high, denom, numer), None)

    start_high = jnp.full((local_rows, key_heads, group), -1e30, jnp.float32)
    start_denom = jnp.zeros((local_rows, key_heads, group), jnp.float32)
    start_numer = jnp.zeros((local_rows, key_heads, group, head_size), jnp.float32)
    carry = (start_high, start_denom, start_numer)
    piece = lax.all_gather(joined, "ep", axis=0, tiled=True)
    length = piece.shape[0]
    size = length
    while size > 2048 and size % 2 == 0:
        size = size // 2
    blocks = piece.reshape(length // size, size, piece.shape[1])
    carry, _ = lax.scan(fold_block, carry, blocks)
    highest, denom, numer = carry
    attended = (
        (numer / denom[..., None]).astype(jnp.bfloat16).reshape(local_rows, query_heads * head_size)
    )
    own_rows = tokens.shape[0]
    width = tokens.shape[1]
    picks_row = route.shape[1]
    experts = lax.axis_size("ep")
    capacity = 2 * own_rows * picks_row // experts
    token_float = tokens.astype(jnp.float32)
    normed = (
        token_float
        * lax.rsqrt(jnp.mean(token_float * token_float, axis=-1, keepdims=True) + EPS)
        * ffn_gain
    ).astype(jnp.bfloat16)
    flat_route = route.reshape(-1)
    expert_hot = (flat_route[:, None] == jnp.arange(experts, dtype=jnp.int32)[None, :]).astype(
        jnp.int32
    )
    earlier = jnp.cumsum(expert_hot, axis=0) - expert_hot
    rank = jnp.sum(earlier * expert_hot, axis=1)
    slot = flat_route * capacity + rank
    pick_hot = (slot[:, None] == jnp.arange(experts * capacity, dtype=jnp.int32)[None, :]).astype(
        jnp.bfloat16
    )
    row_hot = jnp.sum(pick_hot.reshape(own_rows, picks_row, experts * capacity), axis=1)
    outgoing = jnp.einsum("rs,rd->sd", row_hot, normed, preferred_element_type=jnp.float32).astype(
        jnp.bfloat16
    )
    outgoing = outgoing.reshape(experts, capacity, width)
    gate_local = gate_weight[0]
    up_local = up_weight[0]
    down_local = down_weight[0]
    arrived = lax.all_to_all(outgoing, "ep", split_axis=0, concat_axis=0, tiled=True)
    sources = arrived.shape[0]
    items = arrived.shape[1]
    slot_rows = arrived.reshape(sources * items, width)
    piece = lax.all_gather(slot_rows, "tp", axis=0, tiled=True)
    gate = jnp.dot(piece, gate_local, preferred_element_type=jnp.float32)
    upper = jnp.dot(piece, up_local, preferred_element_type=jnp.float32)
    hidden = (jax.nn.silu(gate) * upper).astype(jnp.bfloat16)
    worked = jnp.dot(hidden, down_local, preferred_element_type=jnp.float32).reshape(
        -1, items, width
    )
    head_partial = jnp.dot(attended, out_weight, preferred_element_type=jnp.float32)
    mixer_sum, expert_sum = (
        lax.psum_scatter(
            head_partial.astype(jnp.bfloat16), "tp", scatter_dimension=0, tiled=True
        ).astype(jnp.float32),
        lax.psum_scatter(worked.astype(jnp.bfloat16), "tp", scatter_dimension=0, tiled=True).astype(
            jnp.float32
        ),
    )
    mixer_out = mixer_sum.astype(jnp.bfloat16)
    home = expert_sum.astype(jnp.bfloat16)
    back = lax.all_to_all(home, "ep", split_axis=0, concat_axis=0, tiled=True)
    copies = jnp.dot(
        pick_hot, back.reshape(experts * capacity, width), preferred_element_type=jnp.float32
    )
    weighted = route_weight[..., None] * copies.reshape(own_rows, picks_row, width)
    mixed = jnp.sum(weighted, axis=1).astype(jnp.bfloat16)
    return (mixer_out, mixed)


def solution(mesh):
    placed = (
        P("ep", "tp"),
        P("ep", "tp"),
        P("ep", "tp"),
        P(),
        P(),
        P("tp", None),
        P(("ep", "tp"), None),
        P(),
        P(("ep", "tp"), None),
        P(("ep", "tp"), None),
        P("ep", None, "tp"),
        P("ep", None, "tp"),
        P("ep", "tp", None),
    )
    return jax.shard_map(
        local,
        mesh=mesh,
        in_specs=placed,
        out_specs=(P(("ep", "tp"), None), P(("ep", "tp"), None)),
        check_vma=False,
    )
```

profile of v0, /device:TPU:0, one launch (start us, length us, event | category | flops | bytes accessed | tf_op | source)
XLA Modules:
  0.0 136.9 jit_solution(23721503916896512)
XLA Ops:
  7.2 0.8 copy.46
  8.1 0.1 eq.54
  8.2 0.1 reduce_window_sum.11
  8.3 0.2 select_reduce_fusion
  8.5 0.1 reduce_sum.73
  8.6 0.1 copy.47
  8.7 0.7 multiply_add_fusion
  9.4 0.1 fusion.47
  9.5 1.0 fusion.30
  10.5 1.3 convolution_convert_fusion.1
  11.8 21.7 %all_to_all.10 = bf16[8,16,2048]{2,1,0:T(8,128)(2,1)} all-to-all(bf16[8,16,2048]{2,1,0:T(8,128)(2,1)S(1)} %bitcast.99), channel_id=1, replica_groups=mesh['ep'=8,'tp'=4] {'ep'}, dimensions={0} | all-to-all | bytes 1048576 | tf_op jit(solution)/shard_map/all_to_all | solution.py:130
  33.6 1.0 copy.44
  34.6 0.1 reshape.448
  34.7 0.8 mul.273
  35.6 0.2 multiply_multiply_fusion
  35.8 19.5 %all-gather.2.cloned.1.call-done = bf16[512,2048]{1,0:T(8,128)(2,1)} async-done(((bf16[128,2048]{1,0:T(8,128)(2,1)}), bf16[512,2048]{1,0:T(8,128)(2,1)}) %all-gather.2.cloned.1.call-update) | async-done | bytes 2097168 | tf_op jit(solution)/shard_map/all_gather | solution.py:134
  55.3 5.1 %fusion.10 = f32[512,896]{1,0:T(8,128)S(1)} fusion(bf16[512,2048]{1,0:T(8,128)(2,1)} %all-gather.2.cloned.1.call-done, bf16[1,2048,896]{2,1,0:T(8,128)(2,1)} %param.23), kind=kOutput, calls=%fused_computation.11 | convolution fusion | flops 1879048192 | bytes 7602176 | tf_op jit(solution)/shard_map/dot_general | solution.py:135
  60.5 2.4 %multiply_convert_fusion = bf16[512,896]{1,0:T(8,128)(2,1)S(1)} fusion(f32[512,896]{1,0:T(8,128)S(1)} %fusion.10, bf16[512,2048]{1,0:T(8,128)(2,1)S(1)} %copy-done.7, bf16[1,2048,896]{2,1,0:T(8,128)(2,1)S(1)} %copy-done.5), kind=kOutput, calls=%fused_computation.17 | convolution fusion | flops 1881800704 | bytes 8519680 | tf_op jit(solution)/shard_map/dot_general | solution.py:136
  62.9 3.7 %fusion.12 = bf16[32,16,2048]{2,1,0:T(8,128)(2,1)} fusion(bf16[32,16,896]{2,1,0:T(8,128)(2,1)S(1)} %bitcast.101, bf16[1,896,2048]{2,1,0:T(8,128)(2,1)S(1)} %copy-done.6), kind=kOutput, calls=%fused_computation.13 | convolution fusion | flops 1880096768 | bytes 6684672 | tf_op jit(solution)/shard_map/dot_general | solution.py:138
  66.8 0.1 fusion.44
  66.9 0.3 subtract_convert_fusion
  67.3 0.3 pad_maximum_fusion
  67.7 0.1 fusion.38
  67.8 0.1 subtract_convert_fusion.1
  68.1 31.6 %all_gather.6 = bf16[2048,128]{0,1:T(8,128)(2,1)S(1)} all-gather(bf16[256,128]{0,1:T(8,128)(2,1)S(1)} %pad_maximum_fusion.1), channel_id=1, replica_groups=mesh['ep'=8,'tp'=4] {'ep'}, dimensions={0}, use_global_device_ids=true | all-gather | bytes 589824 | tf_op jit(solution)/shard_map/all_gather | solution.py:90
  99.7 1.3 bitcast_reduce_fusion
  101.0 1.4 %fusion.1 = f32[256,4]{0,1:T(4,128)S(1)} fusion(f32[2048,256,4]{1,0,2:T(8,128)S(1)} %get-tuple-element.37, f32[256,4]{0,1:T(4,128)S(1)} %broadcast_maximum_fusion), kind=kLoop, calls=%fused_computation.3 | loop fusion | flops 6290432 | bytes 8396800 | tf_op jit(solution)/shard_map/while/body/eval_jaxpr/reduce_sum | solution.py:77
  102.4 1.5 %fusion.27 = bf16[1,64,256,4]{2,1,3,0:T(8,128)(2,1)S(1)} fusion(f32[2048,256,4]{1,0,2:T(8,128)S(1)} %get-tuple-element.37, f32[256,4]{0,1:T(4,128)S(1)} %broadcast_maximum_fusion, bf16[2048,128]{0,1:T(8,128)(2,1)S(1)} %all_gather.6, f32[256,4]{0,1:T(4,128)S(1)} %get-tuple-element.29, f32[256,4]{0,1:T(4,128)S(1)} %get-tuple-element.28), kind=kOutput, calls=%fused_computation.22 | convolution fusion | flops 274923520 | bytes 8794112 | tf_op jit(solution)/shard_map/while/body/eval_jaxpr/qkgs,skd->qkgd/dot_general | solution.py:78
  104.0 1.4 %convolution_convert_fusion = bf16[256,2048]{1,0:T(8,128)(2,1)} fusion(bf16[256,256]{0,1:T(8,128)(2,1)S(1)} %bitcast.100, bf16[256,2048]{1,0:T(8,128)(2,1)S(1)} %copy-done), kind=kOutput, calls=%fused_computation.14 | convolution fusion | flops 268959744 | bytes 2228224 | tf_op jit(solution)/shard_map/dot_general | solution.py:141
  105.5 15.8 %all_to_all.11 = bf16[8,16,2048]{2,1,0:T(8,128)(2,1)S(1)} all-to-all(bf16[8,16,2048]{2,1,0:T(8,128)(2,1)} %reduce-scatter.5.cloned.1.call-done), channel_id=1, replica_groups=mesh['ep'=8,'tp'=4] {'ep'}, dimensions={0} | all-to-all | bytes 1048576 | tf_op jit(solution)/shard_map/all_to_all | solution.py:152
  121.3 0.9 fusion.17
  122.2 8.1 %reduce-scatter.3.cloned.1.call-done = bf16[64,2048]{1,0:T(8,128)(2,1)} async-done(((bf16[256,2048]{1,0:T(8,128)(2,1)}), bf16[64,2048]{1,0:T(8,128)(2,1)}) %reduce-scatter.3.cloned.1.call-update) | async-done | bytes 262160 | tf_op jit(solution)/shard_map/reduce_scatter | solution.py:143
  (41 shorter events, 0.7 us)
Async XLA Ops:
  7.2 96.8 %copy-start = (bf16[256,2048]{1,0:T(8,128)(2,1)S(1)}, bf16[256,2048]{1,0:T(8,128)(2,1)}, u32[]{:S(2)}) copy-start(bf16[256,2048]{1,0:T(8,128)(2,1)} %param.18) | copy-start | bytes 3145732
  7.2 48.1 %all-gather.2.cloned.1.call-start = ((), (), s32[]{:S(2)}) async-start(), calls=%async_computation.5 | async-start | bytes 2621440 | tf_op jit(solution)/shard_map/all_gather | solution.py:134
  33.5 71.9 %reduce-scatter.5.cloned.1.call-start = ((), (), s32[]{:S(2)}) async-start(), calls=%async_computation.6 | async-start | bytes 2621440 | tf_op jit(solution)/shard_map/reduce_scatter | solution.py:146
  55.3 5.2 %copy-start.5 = (bf16[1,2048,896]{2,1,0:T(8,128)(2,1)S(1)}, bf16[1,2048,896]{2,1,0:T(8,128)(2,1)}, u32[]{:S(2)}) copy-start(bf16[1,2048,896]{2,1,0:T(8,128)(2,1)} %param.24) | copy-start | bytes 11010052
  55.3 5.2 %copy-start.7 = (bf16[512,2048]{1,0:T(8,128)(2,1)S(1)}, bf16[512,2048]{1,0:T(8,128)(2,1)}, u32[]{:S(2)}) copy-start(bf16[512,2048]{1,0:T(8,128)(2,1)} %all-gather.2.cloned.1.call-done) | copy-start | bytes 6291460
  60.5 2.4 %copy-start.6 = (bf16[1,896,2048]{2,1,0:T(8,128)(2,1)S(1)}, bf16[1,896,2048]{2,1,0:T(8,128)(2,1)}, u32[]{:S(2)}) copy-start(bf16[1,896,2048]{2,1,0:T(8,128)(2,1)} %param.25) | copy-start | bytes 11010052
  62.9 4.7 %copy-start.1 = (bf16[256,64]{0,1:T(8,128)(2,1)S(1)}, bf16[256,64]{0,1:T(8,128)(2,1)}, u32[]{:S(2)}) copy-start(bf16[256,64]{0,1:T(8,128)(2,1)} %param.14) | copy-start | bytes 98308
  62.9 4.7 %copy-start.4 = (f32[64]{0:T(128)S(1)}, f32[64]{0:T(128)}, u32[]{:S(2)}) copy-start(f32[64]{0:T(128)} %param.17) | copy-start | bytes 772
  66.6 1.5 %copy-start.2 = (bf16[256,64]{0,1:T(8,128)(2,1)S(1)}, bf16[256,64]{0,1:T(8,128)(2,1)}, u32[]{:S(2)}) copy-start(bf16[256,64]{0,1:T(8,128)(2,1)} %param.15) | copy-start | bytes 98308
  66.6 63.7 %reduce-scatter.3.cloned.1.call-start = ((), (), s32[]{:S(2)}) async-start(), calls=%async_computation.4 | async-start | bytes 1310720 | tf_op jit(solution)/shard_map/reduce_scatter | solution.py:143
  103.9 17.3 %copy-start.3 = (f32[32,2]{0,1:T(2,128)S(1)}, f32[32,2]{0,1:T(2,128)}, u32[]{:S(2)}) copy-start(f32[32,2]{0,1:T(2,128)} %param.22) | copy-start | bytes 772
Sparse Core Ops, SparseCore 0:
  33.7 21.5 all-gather.1
  66.8 31.1 reduce-scatter.4
  105.6 24.7 reduce-scatter.2
where the time goes:
time: 137 us
  blocking collectives  69.1 us (50%)
  waiting for transfers between devices  27.7 us (20%)
  matrix products  17.7 us (13%)
  between operations  14 us (10%)
  other arithmetic  4.93 us (4%)
  local copies, waits for them, and re-layouts  3.26 us (2%)
    all_gather x1, blocking collectives, local(): piece = lax.all_gather(joined, 'ep', axis=0, tiled=True)  31.6 us
    all_to_all x1, blocking collectives, local(): lax.all_to_all(outgoing, 'ep', split_axis=0, concat_axis=0, tiled=True)  21.7 us
    all_gather x1, waiting for transfers between devices, local(): piece = lax.all_gather(slot_rows, 'tp', axis=0, tiled=True)  19.5 us
    all_to_all x1, blocking collectives, local(): back = lax.all_to_all(home, 'ep', split_axis=0, concat_axis=0, tiled=True)  15.8 us
    reduce_scatter x1, waiting for transfers between devices, local(): lax.psum_scatter(head_partial.astype(jnp.bfloat16), 'tp', scatter_dimensi...  8.13 us
    dot_general x1, matrix products, local(): gate = jnp.dot(piece, gate_local, preferred_element_type=jnp.float32)  5.14 us
    dot_general x1, matrix products, local(): jnp.dot(hidden, down_local, preferred_element_type=jnp.float32)  3.69 us
  transfers between devices with their start and end apart: 3, of which 2 were waited for; matrix products, arithmetic and copies ran while one was open for 7% of the time, Pallas kernels for 0%

commit v1 on v0

v1 whole, which is shorter than its diff:
```python
import functools

import jax
import jax.numpy as jnp
import numpy as np
from jax import lax
from jax.experimental import pallas as pl
from jax.experimental.pallas import tpu as pltpu
from jax.sharding import Mesh
from jax.sharding import PartitionSpec as P

GRID_W = 64
EPS = 1e-06
THETA = 10000.0
LANES = 128
DIRECT_MAX = 8
FLOPS_PER_MICRO = 5e8

WHOLE = "whole"
VMEM = pl.BlockSpec(memory_space=pltpu.VMEM)
SMEM = pl.BlockSpec(memory_space=pltpu.SMEM)
ANY = pl.BlockSpec(memory_space=pltpu.HBM)
MIB = 1024 * 1024


def in_hbm(vals):
    return pltpu.with_memory_space_constraint(vals, pltpu.HBM)


def call(body, outs, in_specs, args, scratch=(), micros=1.0, mib=6):
    def whole(shape):
        return pl.BlockSpec(shape, lambda i: (0,) * len(shape))

    return pl.pallas_call(
        body,
        grid=(1,),
        out_shape=[jax.ShapeDtypeStruct(s, d) for s, d in outs],
        in_specs=[whole(a.shape) if t is WHOLE else t for t, a in zip(in_specs, args)],
        out_specs=[VMEM for _ in outs],
        scratch_shapes=list(scratch),
        compiler_params=pltpu.CompilerParams(vmem_limit_bytes=mib * MIB),
        cost_estimate=pl.CostEstimate(
            flops=int(micros * FLOPS_PER_MICRO), bytes_accessed=0, transcendentals=0
        ),
    )(*[in_hbm(a) if t is WHOLE or t is ANY else a for t, a in zip(in_specs, args)])


def swap(vals, axis, distance=1):
    size = lax.axis_size(axis)
    return lax.ppermute(vals, axis, [(i, i ^ distance) for i in range(size)])


def exchange(vals, capacity):
    shape = vals.shape
    vals = vals.reshape(-1, capacity, shape[1])
    vals = lax.all_to_all(vals, ("n", "y"), split_axis=0, concat_axis=0, tiled=True)
    return vals.reshape(shape)


def pick_hots(meta, base, near, sides, capacity, top):
    rows = meta.shape[0]
    lane = lax.broadcasted_iota(jnp.int32, (rows, LANES), 1).astype(jnp.float32)
    chosen = [meta[:, k : k + 1] for k in range(top)]
    hots = [(c == lane).astype(jnp.float32) for c in chosen]
    count = functools.reduce(jnp.add, hots)
    lower = (
        lax.broadcasted_iota(jnp.int32, (rows, rows), 0)
        > lax.broadcasted_iota(jnp.int32, (rows, rows), 1)
    ).astype(jnp.float32)
    prior = jnp.dot(lower, count, preferred_element_type=jnp.float32)
    total = near * sides * capacity
    spot = lax.broadcasted_iota(jnp.int32, (rows, total), 1)
    spot = (spot // (sides * capacity) * capacity + spot % capacity).astype(jnp.float32)
    out = []
    for k in range(top):
        rank = jnp.sum(hots[k] * prior, axis=1, keepdims=True)
        for j in range(k):
            rank = rank + (chosen[j] == chosen[k]).astype(jnp.float32)
        own = chosen[k] - base
        inside = (own >= 0.0) & (own < float(near))
        slot = jnp.where(inside, own * float(capacity) + rank, -1.0)
        out.append((slot == spot).astype(jnp.float32))
    return out


def spread(hots, normed):
    row_hot = functools.reduce(jnp.add, hots).astype(jnp.bfloat16)
    out = lax.dot_general(
        row_hot, normed, (((0,), (0,)), ((), ())), preferred_element_type=jnp.float32
    )
    return out.astype(jnp.bfloat16)


def send_body(base_ref, tok_ref, gain_ref, route_ref, weight_ref, far_ref, near_ref, *, sizes):
    top = sizes[-1]
    width = tok_ref.shape[1]
    own = tok_ref.shape[0]
    eye = lax.broadcasted_iota(jnp.int32, (own, own), 0) == lax.broadcasted_iota(
        jnp.int32, (own, own), 1
    )

    def column(row):
        return jnp.sum(jnp.where(eye, row, 0.0), axis=1, keepdims=True)

    vals = tok_ref[...].astype(jnp.float32)
    normed = vals * lax.rsqrt(jnp.mean(vals * vals, axis=-1, keepdims=True) + EPS) * gain_ref[...]
    normed = normed.astype(jnp.bfloat16)
    far_ref[:, :width] = normed
    lane = lax.broadcasted_iota(jnp.int32, (vals.shape[0], LANES), 1)
    meta = jnp.zeros((vals.shape[0], LANES), jnp.float32)
    for k in range(top):
        weight = column(weight_ref[k : k + 1, :])
        high = weight.astype(jnp.bfloat16).astype(jnp.float32)
        rest = weight - high
        middle = rest.astype(jnp.bfloat16).astype(jnp.float32)
        pieces = (column(route_ref[k : k + 1, :].astype(jnp.float32)), high, middle, rest - middle)
        for i, piece in enumerate(pieces):
            meta = jnp.where(lane == i * top + k, piece, meta)
    far_ref[:, width:] = meta.astype(jnp.bfloat16)
    hots = pick_hots(meta, base_ref[0].astype(jnp.float32), *sizes)
    near_ref[...] = spread(hots, normed)


def relay_body(base_ref, far_ref, out_ref, *, sizes):
    width = out_ref.shape[1]
    meta = far_ref[:, width:].astype(jnp.float32)
    hots = pick_hots(meta, base_ref[0].astype(jnp.float32), *sizes)
    out_ref[...] = spread(hots, far_ref[:, :width])


def collect_body(base_ref, meta_ref, back_ref, out_ref, *, sizes):
    top = sizes[-1]
    meta = meta_ref[:, out_ref.shape[1] :].astype(jnp.float32)
    hots = pick_hots(meta, base_ref[0].astype(jnp.float32), *sizes)
    back = back_ref[...]
    total = None
    for k in range(top):
        rows = jnp.dot(hots[k].astype(jnp.bfloat16), back, preferred_element_type=jnp.float32)
        rows = rows.astype(jnp.bfloat16).astype(jnp.float32)
        weight = meta[:, top + k : top + k + 1] + (
            meta[:, 2 * top + k : 2 * top + k + 1] + meta[:, 3 * top + k : 3 * top + k + 1]
        )
        total = weight * rows if total is None else total + weight * rows
    out_ref[...] = total.astype(out_ref.dtype)


def expert_body(
    mine_ref, other_ref, gate_hbm, up_hbm, down_hbm, mine_out, other_out, gate, up, down, sems
):
    copies = [
        pltpu.make_async_copy(src.at[0], dst, sems.at[i])
        for i, (src, dst) in enumerate(((gate_hbm, gate), (up_hbm, up), (down_hbm, down)))
    ]
    for copy in copies:
        copy.start()
    rows = jnp.concatenate([mine_ref[...], other_ref[...]], axis=0)
    count = mine_ref.shape[0]
    copies[0].wait()
    lhs = jnp.dot(rows, gate[...], preferred_element_type=jnp.float32)
    copies[1].wait()
    rhs = jnp.dot(rows, up[...], preferred_element_type=jnp.float32)
    hidden = (lhs / (1.0 + jnp.exp(-lhs)) * rhs).astype(jnp.bfloat16)
    copies[2].wait()
    out = jnp.dot(hidden, down[...], preferred_element_type=jnp.float32).astype(jnp.bfloat16)
    mine_out[...] = out[:count]
    other_out[...] = out[count:]


def add_body(left_ref, right_ref, out_ref):
    total = left_ref[...].astype(jnp.float32) + right_ref[...].astype(jnp.float32)
    out_ref[...] = total.astype(out_ref.dtype)


def run_expert(mine, other, gate_weight, up_weight, down_weight):
    count, width = mine.shape
    inner = gate_weight.shape[2]
    bf16 = jnp.bfloat16
    return call(
        expert_body,
        [((count, width), bf16), ((count, width), bf16)],
        [VMEM, VMEM, ANY, ANY, ANY],
        (mine, other, gate_weight, up_weight, down_weight),
        [
            pltpu.VMEM((width, inner), bf16),
            pltpu.VMEM((width, inner), bf16),
            pltpu.VMEM((inner, width), bf16),
            pltpu.SemaphoreType.DMA((3,)),
        ],
        micros=5.0,
        mib=24,
    )


def turn_tables(rows_total, head_size):
    quarter = head_size // 4
    freqs = THETA ** (-np.arange(quarter, dtype=np.float64) / quarter)
    sign = np.where(np.arange(head_size // 2) % 2 == 0, -1.0, 1.0)

    def table(count, first):
        angle = np.repeat(np.arange(count, dtype=np.float64)[:, None] * freqs, 2, axis=1)
        zero = np.zeros_like(angle)
        out = []
        for part in (np.cos(angle), np.sin(angle) * sign):
            halves = [part, zero] if first else [zero, part]
            out.append(np.concatenate(halves, axis=1))
        return np.stack(out).astype(np.float32)

    return table(rows_total, True), table(GRID_W, False)


def qkv_body(start_ref, q_ref, k_ref, v_ref, qg_ref, kg_ref, row_ref, col_ref, _, q_out, kv_out):
    rows, q_width = q_ref.shape
    k_width = k_ref.shape[0]
    head = qg_ref.shape[1]
    span = q_width + k_width
    unit = (
        lax.broadcasted_iota(jnp.int32, (k_width, k_width), 0)
        == lax.broadcasted_iota(jnp.int32, (k_width, k_width), 1)
    ).astype(jnp.bfloat16)

    def upright(ref):
        return lax.dot_general(
            ref[...], unit, (((0,), (0,)), ((), ())), preferred_element_type=jnp.float32
        )

    vals = jnp.concatenate([q_ref[...].astype(jnp.float32), upright(k_ref)], axis=1)
    gain = jnp.concatenate([qg_ref[...]] * (q_width // head) + [kg_ref[...]] * (k_width // head), 1)
    same = (
        lax.broadcasted_iota(jnp.int32, (span, span), 0) // head
        == lax.broadcasted_iota(jnp.int32, (span, span), 1) // head
    ).astype(jnp.float32)
    power = jnp.dot(
        vals * vals, same, preferred_element_type=jnp.float32, precision=lax.Precision.HIGHEST
    )
    vals = vals * lax.rsqrt(power * (1.0 / head) + EPS) * gain
    even = lax.broadcasted_iota(jnp.int32, (rows, span), 1) % 2 == 0
    left = jnp.concatenate([vals[:, 1:], vals[:, :1]], axis=1)
    right = jnp.concatenate([vals[:, span - 1 :], vals[:, : span - 1]], axis=1)
    partner = jnp.where(even, left, right)
    turned = []
    for i in range(rows // GRID_W):
        at = start_ref[0] + i
        cosine = row_ref[0, pl.ds(at, 1), :] + col_ref[0]
        sine = row_ref[1, pl.ds(at, 1), :] + col_ref[1]
        cosine = jnp.concatenate([cosine] * (span // head), axis=1)
        sine = jnp.concatenate([sine] * (span // head), axis=1)
        low = i * GRID_W
        high = low + GRID_W
        turned.append(vals[low:high] * cosine + partner[low:high] * sine)
    turned = jnp.concatenate(turned, axis=0).astype(jnp.bfloat16)
    q_out[...] = turned[:, :q_width] * (head**-0.5)
    kv_out[...] = jnp.concatenate(
        [turned[:, q_width:], upright(v_ref).astype(jnp.bfloat16)], axis=1
    )


def attend_body(core_ref, q_ref, *refs, head, key_heads, sides):
    kvs = refs[:-4]
    weight_ref, sent_ref, kept_ref, att = refs[-4:]
    heads = q_ref.shape[1] // head
    for h in range(heads):
        g = h * key_heads // heads
        query = q_ref[:, h * head : (h + 1) * head]
        scores = []
        for kv in kvs:
            scores.append(
                lax.dot_general(
                    query,
                    kv[:, g * head : (g + 1) * head],
                    (((1,), (1,)), ((), ())),
                    preferred_element_type=jnp.float32,
                )
            )
        high = functools.reduce(jnp.maximum, [jnp.max(s, -1, keepdims=True) for s in scores])
        denom = None
        numer = None
        for s, kv in zip(scores, kvs):
            expo = jnp.exp(s - high)
            part = jnp.sum(expo, axis=-1, keepdims=True)
            at = (key_heads + g) * head
            prod = jnp.dot(
                expo.astype(jnp.bfloat16), kv[:, at : at + head], preferred_element_type=jnp.float32
            )
            denom = part if denom is None else denom + part
            numer = prod if numer is None else numer + prod
        att[:, h * head : (h + 1) * head] = (numer / denom).astype(jnp.bfloat16)
    share = q_ref.shape[0] // (2 * sides)
    core = core_ref[0]
    for out_ref, which in ((sent_ref, 1 - core), (kept_ref, core)):
        rows = jnp.concatenate(
            [att[pl.ds(pl.multiple_of((2 * s + which) * share, share), share), :] for s in range(sides)]
        )
        out = jnp.dot(rows, weight_ref[...], preferred_element_type=jnp.float32)
        out_ref[...] = out.astype(jnp.bfloat16)


def attend_blocks(rot_q, joined, key_heads, head):
    rows = rot_q.shape[0]
    group = rot_q.shape[1] // head // key_heads
    queries = rot_q.reshape(rows, key_heads, group, head)
    width = key_heads * head

    def fold_block(carry, block):
        highest, denom, numer = carry
        key_block = block[:, :width].reshape(-1, key_heads, head)
        value_block = block[:, width:].reshape(-1, key_heads, head)
        scores = jnp.einsum("qkgd,skd->qkgs", queries, key_block, preferred_element_type=jnp.float32)
        new_high = jnp.maximum(highest, jnp.max(scores, axis=-1))
        shrink = jnp.exp(highest - new_high)
        expo = jnp.exp(scores - new_high[..., None])
        denom = denom * shrink + jnp.sum(expo, axis=-1)
        numer = numer * shrink[..., None] + jnp.einsum(
            "qkgs,skd->qkgd",
            expo.astype(jnp.bfloat16),
            value_block,
            preferred_element_type=jnp.float32,
        )
        return ((new_high, denom, numer), None)

    shape = (rows, key_heads, group)
    carry = (
        jnp.full(shape, -1e30, jnp.float32),
        jnp.zeros(shape, jnp.float32),
        jnp.zeros(shape + (head,), jnp.float32),
    )
    length = joined.shape[0]
    size = length
    while size > 2048 and size % 2 == 0:
        size = size // 2
    blocks = joined.reshape(length // size, size, joined.shape[1])
    carry, _ = lax.scan(fold_block, carry, blocks)
    _, denom, numer = carry
    return (numer / denom[..., None]).astype(jnp.bfloat16).reshape(rows, -1)


def attention(rot_q, joined, out_weight, key_heads, head):
    near = lax.axis_size("n")
    sides = lax.axis_size("y")
    core = lax.axis_index("c").astype(jnp.int32)
    rows = rot_q.shape[0]
    width = out_weight.shape[1]
    far = swap(joined, "f")
    if near <= DIRECT_MAX:
        pair = jnp.concatenate([joined, far], axis=0)
        kvs = [pair] + [swap(pair, "n", k) for k in range(1, near)]
        body = functools.partial(attend_body, head=head, key_heads=key_heads, sides=sides)
        half = ((rows // 2, width), jnp.bfloat16)
        return call(
            body,
            [half, half],
            [SMEM] + [VMEM] * (len(kvs) + 1) + [WHOLE],
            (core.reshape(1), rot_q, *kvs, out_weight),
            [pltpu.VMEM(rot_q.shape, jnp.bfloat16)],
            micros=5.0,
            mib=24,
        )
    pair = jnp.concatenate([joined, far], axis=0)
    joined = lax.all_gather(pair, "n", axis=0, tiled=True)
    attended = attend_blocks(rot_q, joined, key_heads, head)
    blocks = attended.reshape(sides, 2, -1, attended.shape[1])

    def project(which):
        part = lax.dynamic_index_in_dim(blocks, which, 1, False).reshape(rows // 2, -1)
        out = jnp.dot(part, out_weight, preferred_element_type=jnp.float32)
        return out.astype(jnp.bfloat16)

    return project(1 - core), project(core)


def finish_mixer(sent, kept):
    sides = lax.axis_size("y")
    pair = kept.astype(jnp.float32) + swap(sent, "c").astype(jnp.float32)
    pair = pair.reshape(sides, -1, kept.shape[1])
    if sides == 1:
        return pair[0].astype(jnp.bfloat16)
    if sides == 2:
        side = lax.axis_index("y")
        sent = lax.dynamic_index_in_dim(pair, 1 - side, 0, False).astype(jnp.bfloat16)
        kept = lax.dynamic_index_in_dim(pair, side, 0, False)
        return (kept + swap(sent, "y").astype(jnp.float32)).astype(jnp.bfloat16)
    moved = lax.all_to_all(pair.astype(jnp.bfloat16), "y", 0, 0, tiled=True)
    return jnp.sum(moved.astype(jnp.float32), axis=0).astype(jnp.bfloat16)


def local(
    queries,
    keys,
    values,
    q_gain,
    k_gain,
    out_weight,
    tokens,
    ffn_gain,
    route,
    route_weight,
    gate_weight,
    up_weight,
    down_weight,
):
    bf16 = jnp.bfloat16
    near = lax.axis_size("n")
    sides = lax.axis_size("y")
    half = lax.axis_index("f").astype(jnp.int32)
    here = half * near + lax.axis_index("n").astype(jnp.int32)
    base = (half * near).reshape(1)

    own_rows, width = tokens.shape
    top = route.shape[1]
    capacity = own_rows * top // near
    sizes = (near, sides, capacity, top)
    slots = near * sides * capacity
    send = functools.partial(send_body, sizes=sizes)
    outgoing, near_rows = call(
        send, [((own_rows, width + LANES), bf16), ((slots, width), bf16)], [SMEM] + [WHOLE] * 4,
        (base, tokens, ffn_gain.reshape(1, -1), route.T, route_weight.T), micros=1.5)
    far = swap(outgoing, "f")
    near_in = exchange(near_rows, capacity)
    relay = functools.partial(relay_body, sizes=sizes)
    (far_rows,) = call(relay, [((slots, width), bf16)], [SMEM, VMEM], (base, far))
    far_in = exchange(far_rows, capacity)

    local_rows = queries.shape[0]
    head = q_gain.shape[0]
    row_table, col_table = turn_tables(local_rows * 2 * near // GRID_W, head)
    rot_q, joined = call(
        qkv_body,
        [(queries.shape, bf16), ((local_rows, 2 * keys.shape[1]), bf16)],
        [SMEM] + [WHOLE] * 7 + [VMEM],
        (
            (here * (local_rows // GRID_W)).reshape(1),
            queries,
            keys.T,
            values.T,
            q_gain.reshape(1, -1),
            k_gain.reshape(1, -1),
            row_table,
            col_table,
            near_rows,
        ),
        micros=1.5,
    )

    weights = (gate_weight, up_weight, down_weight)

    def work(rows):
        mine, other = run_expert(rows, swap(rows, "c"), *weights)
        args = (mine, swap(other, "c"))
        return call(add_body, [(rows.shape, bf16)], [VMEM] * 2, args)[0]

    near_out = work(near_in)
    far_out = work(far_in)
    far_back = exchange(far_out, capacity)
    near_back = exchange(near_out, capacity)

    sent, kept = attention(rot_q, joined, out_weight, keys.shape[1] // head, head)
    mixer_out = finish_mixer(sent, kept)

    collect = functools.partial(collect_body, sizes=sizes)

    def gather_back(meta, back, dtype):
        return call(
            collect, [((own_rows, width), dtype)], [SMEM, VMEM, VMEM], (base, meta, back)
        )[0]

    far_sum = swap(gather_back(far, far_back, bf16), "f")
    near_sum = gather_back(outgoing, near_back, jnp.float32)
    mixed = (near_sum + far_sum.astype(jnp.float32)).astype(bf16)
    return (mixer_out, mixed)


def solution(mesh):
    devices = mesh.devices
    groups, parts = devices.shape
    split = Mesh(devices.reshape(2, groups // 2, parts // 2, 2), ("f", "n", "y", "c"))
    ep = ("f", "n")
    tp = ("y", "c")
    placed = (
        P(ep, tp),
        P(ep, tp),
        P(ep, tp),
        P(),
        P(),
        P(tp, None),
        P(ep + tp, None),
        P(),
        P(ep + tp, None),
        P(ep + tp, None),
        P(ep, None, tp),
        P(ep, None, tp),
        P(ep, tp, None),
    )
    return jax.shard_map(
        local,
        mesh=split,
        in_specs=placed,
        out_specs=(P(ep + tp, None), P(ep + tp, None)),
        check_vma=False,
    )
```

time: 137 us -> 101 us (0.74)
  blocking collectives: 69.1 us -> 13.3 us
  Pallas kernels: 0 us -> 26.6 us
  starting transfers between devices: 0.12 us -> 26.5 us
  matrix products: 17.7 us -> 0 us
  between operations: 14 us -> 0.76 us
  waiting for transfers between devices: 27.7 us -> 22.6 us
  local copies, waits for them, and re-layouts: 3.26 us -> 6.65 us
    all_gather x1 -> x0, blocking collectives: 31.6 us -> none  [local(): piece = lax.all_gather(joined, 'ep', axis=0, tiled=True)]
    pallas_call x0 -> x10, Pallas kernels: none -> 26.6 us  [call(): pl.pallas_call(body, grid=(1,), out_shape=[jax.ShapeDtypeStruct(s, d) for...]
    all_to_all x2 -> x1, blocking collectives: 37.5 us -> 13.3 us  [exchange(): lax.all_to_all(vals, ('n', 'y'), split_axis=0, concat_axis=0, tiled=True)]
    ppermute x0 -> x12, waiting for transfers between devices: none -> 22.1 us  [swap(): return lax.ppermute(vals, axis, [(i, i ^ distance) for i in range(size)])]
    all_gather x1 -> x0, waiting for transfers between devices: 19.5 us -> none  [local(): piece = lax.all_gather(slot_rows, 'tp', axis=0, tiled=True)]
    dot_general x8 -> x0, matrix products: 17.7 us -> none  [the longest x1 5.14 us: local(): gate = jnp.dot(piece, gate_local, preferred_element_type=jnp.float32)]
    ppermute x0 -> x12, starting transfers between devices: none -> 13.8 us  [swap(): return lax.ppermute(vals, axis, [(i, i ^ distance) for i in range(size)])]
    all_to_all x0 -> x3, starting transfers between devices: none -> 12.7 us  [exchange(): lax.all_to_all(vals, ('n', 'y'), split_axis=0, concat_axis=0, tiled=True)]
  transfers between devices with their start and end apart: 3 -> 15, of which waited for: 2 -> 6; matrix products, arithmetic and copies ran while one was open for 7% -> 4% of each run, Pallas kernels for 0% -> 23%
where the time goes in v1:
time: 101 us; the launch traced here: 100 us
  Pallas kernels  26.6 us (26%)
  starting transfers between devices  26.5 us (26%)
  waiting for transfers between devices  22.6 us (22%)
  blocking collectives  13.3 us (13%)
  local copies, waits for them, and re-layouts  6.65 us (7%)
  other arithmetic  3.59 us (4%)
    pallas_call x10, Pallas kernels, call(): pl.pallas_call(body, grid=(1,), out_shape=[jax.ShapeDtypeStruct(s, d) for...  26.6 us
    ppermute x12, waiting for transfers between devices, swap(): return lax.ppermute(vals, axis, [(i, i ^ distance) for i in range(size)])  22.1 us
    ppermute x12, starting transfers between devices, swap(): return lax.ppermute(vals, axis, [(i, i ^ distance) for i in range(size)])  13.8 us
    all_to_all x1, blocking collectives, exchange(): lax.all_to_all(vals, ('n', 'y'), split_axis=0, concat_axis=0, tiled=True)  13.3 us
    all_to_all x3, starting transfers between devices, exchange(): lax.all_to_all(vals, ('n', 'y'), split_axis=0, concat_axis=0, tiled=True)  12.7 us
    unnamed x19, local copies, waits for them, and re-layouts  5.57 us
    add x1, other arithmetic, finish_mixer(): pair = kept.astype(jnp.float32) + swap(sent, 'c').astype(jnp.float32)  2.15 us
  transfers between devices with their start and end apart: 15, of which 6 were waited for; matrix products, arithmetic and copies ran while one was open for 4% of the time, Pallas kernels for 23%

profile of v1, /device:TPU:0, one launch (start us, length us, event | category | flops | bytes accessed | tf_op | source)
XLA Modules:
  0.0 100.1 jit_solution(6902016646508915182)
XLA Ops:
  0.6 2.6 %shard_map.158 = (bf16[32,2176]{1,0:T(8,128)(2,1)S(1)}, bf16[128,2048]{1,0:T(8,128)(2,1)}) custom-call(s32[1]{0:T(128)} %bitcast.6.base_ref, bf16[32,2048]{1,0:T(8,128)(2,1)} %tok_ref.1, f32[1,2048]{1,0:T(1,128)} %bitcast.36, s32[2,32]{1,0:T(2,128)} %bitcast.37, f32[2,32]{1,0:T(2,128)} %bitcast.38), custom_call_target="tpu_custom_call" | custom-call | flops 750000000 | tf_op jit(solution)/shard_map/pallas_call | solution.py:34
  3.2 4.1 %collective-permute-start.8 = (bf16[32,2176]{1,0:T(8,128)(2,1)S(1)}, bf16[32,2176]{1,0:T(8,128)(2,1)S(1)}, u32[]{:S(2)}, u32[]{:S(2)}) collective-permute-start(bf16[32,2176]{1,0:T(8,128)(2,1)S(1)} %get-tuple-element.17.meta_ref), channel_id=1, source_target_pairs={{0,16},{16,0},{1,17},{17,1},{2,18},{18,2},{3,19},{19,3},{4,20},{20... | collective-permute-start | bytes 417800 | tf_op jit(solution)/shard_map/ppermute | solution.py:50
  7.3 6.7 %collective-permute-done.8.far_ref.meta_ref = bf16[32,2176]{1,0:T(8,128)(2,1)S(1)} collective-permute-done((bf16[32,2176]{1,0:T(8,128)(2,1)S(1)}, bf16[32,2176]{1,0:T(8,128)(2,1)S(1)}, u32[]{:S(2)}, u32[]{:S(2)}) %collective-permute-start.8) | collective-permute-done | bytes 139296 | tf_op jit(solution)/shard_map/ppermute | solution.py:50
  14.0 0.7 shard_map.164
  14.7 13.3 %all_to_all.20 = bf16[8,16,2048]{2,1,0:T(8,128)(2,1)S(1)} all-to-all(bf16[8,16,2048]{2,1,0:T(8,128)(2,1)S(1)} %bitcast.31), channel_id=1, replica_groups=mesh['f'=2,'n'=4,'y'=2,'c'=2] {'n','y'}, dimensions={0} | all-to-all | bytes 1048576 | tf_op jit(solution)/shard_map/all_to_all | solution.py:56
  28.0 3.5 %all-to-all-start = ((bf16[8,16,2048]{2,1,0:T(8,128)(2,1)}), bf16[8,16,2048]{2,1,0:T(8,128)(2,1)S(1)}, u32[]{:S(2)}, u32[]{:S(2)}) async-start(bf16[8,16,2048]{2,1,0:T(8,128)(2,1)} %bitcast.13), calls=%async_computation | async-start | bytes 1048576 | tf_op jit(solution)/shard_map/all_to_all | solution.py:56
  31.5 2.3 %shard_map.159 = (bf16[256,256]{1,0:T(8,128)(2,1)S(1)}, bf16[256,128]{1,0:T(8,128)(2,1)S(1)}) custom-call(s32[1]{0:T(128)} %bitcast.1.start_ref, bf16[256,256]{1,0:T(8,128)(2,1)} %q_ref.1, bf16[64,256]{1,0:T(8,128)(2,1)} %bitcast.34, bf16[64,256]{1,0:T(8,128)(2,1)} %bitcast.35, f32[1,64]{1,0:T(1,128)} %bitcast.39, f32[1,64]{1,0:T(1,128)} %bitcast.40, ...), custom_call_target="tpu_custom_call" | custom-call | flops 750000000 | tf_op jit(solution)/shard_map/pallas_call | solution.py:34
  33.9 3.4 %collective-permute-start = (bf16[256,128]{1,0:T(8,128)(2,1)S(1)}, bf16[256,128]{1,0:T(8,128)(2,1)S(1)}, u32[]{:S(2)}, u32[]{:S(2)}) collective-permute-start(bf16[256,128]{1,0:T(8,128)(2,1)S(1)} %get-tuple-element.14), channel_id=1, source_target_pairs={{0,16},{16,0},{1,17},{17,1},{2,18},{18,2},{3,19},{19,3},{4,20},{20... | collective-permute-start | bytes 196616 | tf_op jit(solution)/shard_map/ppermute | solution.py:50
  37.3 5.8 %shard_map.165 = (bf16[128,2048]{1,0:T(8,128)(2,1)S(1)}, bf16[128,2048]{1,0:T(8,128)(2,1)S(1)}) custom-call(bf16[128,2048]{1,0:T(8,128)(2,1)S(1)} %bitcast.28, bf16[128,2048]{1,0:T(8,128)(2,1)S(1)} %collective-permute-done.9.other_ref, bf16[1,2048,896]{2,1,0:T(8,128)(2,1)} %gate_hbm.3, bf16[1,2048,896]{2,1,0:T(8,128)(2,1)} %up_hbm.3, ...), custom_call_target="tpu_custom_call" | custom-call | flops 2500000000 | tf_op jit(solution)/shard_map/pallas_call | solution.py:34
  43.5 1.8 %collective-permute-start.1 = (bf16[512,128]{1,0:T(8,128)(2,1)S(1)}, bf16[512,128]{1,0:T(8,128)(2,1)S(1)}, u32[]{:S(2)}, u32[]{:S(2)}) collective-permute-start(bf16[512,128]{1,0:T(8,128)(2,1)S(1)} %constant_dynamic-update-slice_fusion.refs_0_), channel_id=1, source_target_pairs={{0,4},{4,0},{8,12},{12,8},{1,5},{5,1},{9,13},{13,9},{2,6},{6,2},{1... | collective-permute-start | bytes 393224 | tf_op jit(solution)/shard_map/ppermute | solution.py:50
  45.3 1.5 %collective-permute-start.2 = (bf16[512,128]{1,0:T(8,128)(2,1)S(1)}, bf16[512,128]{1,0:T(8,128)(2,1)S(1)}, u32[]{:S(2)}, u32[]{:S(2)}) collective-permute-start(bf16[512,128]{1,0:T(8,128)(2,1)S(1)} %constant_dynamic-update-slice_fusion.refs_0_), channel_id=1, source_target_pairs={{0,8},{4,12},{8,0},{12,4},{1,9},{5,13},{9,1},{13,5},{2,10},{6,14},... | collective-permute-start | bytes 393224 | tf_op jit(solution)/shard_map/ppermute | solution.py:50
  47.1 2.4 %collective-permute-done.1.refs_1_ = bf16[512,128]{1,0:T(8,128)(2,1)S(1)} collective-permute-done((bf16[512,128]{1,0:T(8,128)(2,1)S(1)}, bf16[512,128]{1,0:T(8,128)(2,1)S(1)}, u32[]{:S(2)}, u32[]{:S(2)}) %collective-permute-start.1) | collective-permute-done | bytes 131104 | tf_op jit(solution)/shard_map/ppermute | solution.py:50
  50.1 1.6 %collective-permute-done.2.refs_2_ = bf16[512,128]{1,0:T(8,128)(2,1)S(1)} collective-permute-done((bf16[512,128]{1,0:T(8,128)(2,1)S(1)}, bf16[512,128]{1,0:T(8,128)(2,1)S(1)}, u32[]{:S(2)}, u32[]{:S(2)}) %collective-permute-start.2) | collective-permute-done | bytes 131104 | tf_op jit(solution)/shard_map/ppermute | solution.py:50
  52.3 1.2 %collective-permute-done.3.refs_3_ = bf16[512,128]{1,0:T(8,128)(2,1)S(1)} collective-permute-done((bf16[512,128]{1,0:T(8,128)(2,1)S(1)}, bf16[512,128]{1,0:T(8,128)(2,1)S(1)}, u32[]{:S(2)}, u32[]{:S(2)}) %collective-permute-start.3) | collective-permute-done | bytes 131104 | tf_op jit(solution)/shard_map/ppermute | solution.py:50
  54.1 0.9 copy-done.1
  55.0 0.9 copy-done.3
  55.9 0.9 copy-done.5
  56.8 0.9 copy-done.7
  57.7 6.0 %shard_map.160 = (bf16[128,2048]{1,0:T(8,128)(2,1)}, bf16[128,2048]{1,0:T(8,128)(2,1)S(1)}) custom-call(s32[1]{0:T(128)} %bitcast.core_ref, bf16[256,256]{1,0:T(8,128)(2,1)S(1)} %copy-done.7, bf16[512,128]{1,0:T(8,128)(2,1)S(1)} %constant_dynamic-update-slice_fusion.refs_0_, bf16[512,128]{1,0:T(8,128)(2,1)S(1)} %copy-done.1, bf16[512,128]{1,0:T(8,128)(2,1)S(1)} %copy-done.3, ...), custom_call_target="tpu_custom_call" | custom-call | flops 2500000000 | tf_op jit(solution)/shard_map/pallas_call | solution.py:34
  63.8 0.9 shard_map.166
  64.7 4.8 %all-to-all-start.3 = ((bf16[8,16,2048]{2,1,0:T(8,128)(2,1)}), bf16[8,16,2048]{2,1,0:T(8,128)(2,1)S(1)}, u32[]{:S(2)}, u32[]{:S(2)}) async-start(bf16[8,16,2048]{2,1,0:T(8,128)(2,1)} %bitcast.19), calls=%async_computation.3 | async-start | bytes 1048576 | tf_op jit(solution)/shard_map/all_to_all | solution.py:56
  69.5 5.8 %shard_map.161 = (bf16[128,2048]{1,0:T(8,128)(2,1)S(1)}, bf16[128,2048]{1,0:T(8,128)(2,1)S(1)}) custom-call(bf16[128,2048]{1,0:T(8,128)(2,1)S(1)} %bitcast.26, bf16[128,2048]{1,0:T(8,128)(2,1)S(1)} %collective-permute-done.6.other_ref, bf16[1,2048,896]{2,1,0:T(8,128)(2,1)} %gate_hbm.3, bf16[1,2048,896]{2,1,0:T(8,128)(2,1)} %up_hbm.3, ...), custom_call_target="tpu_custom_call" | custom-call | flops 2500000000 | tf_op jit(solution)/shard_map/pallas_call | solution.py:34
  75.6 2.2 %convert_add_fusion = f32[128,2048]{1,0:T(8,128)} fusion(bf16[128,2048]{1,0:T(8,128)(2,1)} %collective-permute-done.4, bf16[128,2048]{1,0:T(8,128)(2,1)S(1)} %get-tuple-element.15), kind=kLoop, calls=%fused_computation | loop fusion | flops 786432 | bytes 2097152 | tf_op jit(solution)/shard_map/add | solution.py:372
  77.8 0.9 shard_map.162
  79.2 4.4 %all-to-all-start.1 = ((bf16[8,16,2048]{2,1,0:T(8,128)(2,1)}), bf16[8,16,2048]{2,1,0:T(8,128)(2,1)S(1)}, u32[]{:S(2)}, u32[]{:S(2)}) async-start(bf16[8,16,2048]{2,1,0:T(8,128)(2,1)} %bitcast.15), calls=%async_computation.1 | async-start | bytes 1048576 | tf_op jit(solution)/shard_map/all_to_all | solution.py:56
  83.6 1.1 %fusion.1 = bf16[64,2048]{1,0:T(8,128)(2,1)S(1)} fusion(f32[2,64,2048]{2,1,0:T(8,128)} %bitcast.32, s32[]{:T(128)S(6)} %select_n.8), kind=kLoop, calls=%fused_computation.4 | loop fusion | bytes 524292 | tf_op jit(solution)/shard_map/convert_element_type | solution.py:378
  84.7 2.1 %collective-permute-start.5 = (bf16[64,2048]{1,0:T(8,128)(2,1)S(1)}, bf16[64,2048]{1,0:T(8,128)(2,1)S(1)}, u32[]{:S(2)}, u32[]{:S(2)}) collective-permute-start(bf16[64,2048]{1,0:T(8,128)(2,1)S(1)} %fusion.1), channel_id=1, source_target_pairs={{0,2},{2,0},{1,3},{3,1},{4,6},{6,4},{5,7},{7,5},{8,10},{10,8},{9,1... | collective-permute-start | bytes 786440 | tf_op jit(solution)/shard_map/ppermute | solution.py:50
  86.8 0.7 shard_map.167
  87.6 10.3 %collective-permute-done.5 = bf16[64,2048]{1,0:T(8,128)(2,1)S(1)} collective-permute-done((bf16[64,2048]{1,0:T(8,128)(2,1)S(1)}, bf16[64,2048]{1,0:T(8,128)(2,1)S(1)}, u32[]{:S(2)}, u32[]{:S(2)}) %collective-permute-start.5) | collective-permute-done | bytes 262176 | tf_op jit(solution)/shard_map/ppermute | solution.py:50
  97.9 0.7 fusion
  98.7 0.7 shard_map.163
  99.4 0.7 add_convert_fusion
  (33 shorter events, 3.5 us)
Async XLA Ops:
  3.2 10.7 %collective-permute-start.8 = (bf16[32,2176]{1,0:T(8,128)(2,1)S(1)}, bf16[32,2176]{1,0:T(8,128)(2,1)S(1)}, u32[]{:S(2)}, u32[]{:S(2)}) collective-permute-start(bf16[32,2176]{1,0:T(8,128)(2,1)S(1)} %get-tuple-element.17.meta_ref), channel_id=1, source_target_pairs={{0,16},{16,0},{1,17},{17,1},{2,18},{18,2},{3,19},{19,3},{4,20},{20... | collective-permute-start | bytes 417800 | tf_op jit(solution)/shard_map/ppermute | solution.py:50
  28.0 9.3 %collective-permute-start.9 = (bf16[128,2048]{1,0:T(8,128)(2,1)S(1)}, bf16[128,2048]{1,0:T(8,128)(2,1)S(1)}, u32[]{:S(2)}, u32[]{:S(2)}) collective-permute-start(bf16[128,2048]{1,0:T(8,128)(2,1)S(1)} %bitcast.27), channel_id=1, source_target_pairs={{0,1},{1,0},{2,3},{3,2},{4,5},{5,4},{6,7},{7,6},{8,9},{9,8},{10,11... | collective-permute-start | bytes 1572872 | tf_op jit(solution)/shard_map/ppermute | solution.py:50
  28.0 19.0 %all-to-all-start = ((bf16[8,16,2048]{2,1,0:T(8,128)(2,1)}), bf16[8,16,2048]{2,1,0:T(8,128)(2,1)S(1)}, u32[]{:S(2)}, u32[]{:S(2)}) async-start(bf16[8,16,2048]{2,1,0:T(8,128)(2,1)} %bitcast.13), calls=%async_computation | async-start | bytes 1048576 | tf_op jit(solution)/shard_map/all_to_all | solution.py:56
  33.8 9.3 %copy-start.6 = (bf16[256,256]{1,0:T(8,128)(2,1)}, bf16[256,256]{1,0:T(8,128)(2,1)S(1)}, u32[]{:S(2)}) copy-start(bf16[256,256]{1,0:T(8,128)(2,1)S(1)} %get-tuple-element.13.q_ref) | copy-start | bytes 393220
  33.9 9.6 %collective-permute-start = (bf16[256,128]{1,0:T(8,128)(2,1)S(1)}, bf16[256,128]{1,0:T(8,128)(2,1)S(1)}, u32[]{:S(2)}, u32[]{:S(2)}) collective-permute-start(bf16[256,128]{1,0:T(8,128)(2,1)S(1)} %get-tuple-element.14), channel_id=1, source_target_pairs={{0,16},{16,0},{1,17},{17,1},{2,18},{18,2},{3,19},{19,3},{4,20},{20... | collective-permute-start | bytes 196616 | tf_op jit(solution)/shard_map/ppermute | solution.py:50
  43.2 20.6 %collective-permute-start.10 = (bf16[128,2048]{1,0:T(8,128)(2,1)S(1)}, bf16[128,2048]{1,0:T(8,128)(2,1)S(1)}, u32[]{:S(2)}, u32[]{:S(2)}) collective-permute-start(bf16[128,2048]{1,0:T(8,128)(2,1)S(1)} %get-tuple-element.21), channel_id=1, source_target_pairs={{0,1},{1,0},{2,3},{3,2},{4,5},{5,4},{6,7},{7,6},{8,9},{9,8},{10,11... | collective-permute-start | bytes 1572872 | tf_op jit(solution)/shard_map/ppermute | solution.py:50
  43.5 5.9 %collective-permute-start.1 = (bf16[512,128]{1,0:T(8,128)(2,1)S(1)}, bf16[512,128]{1,0:T(8,128)(2,1)S(1)}, u32[]{:S(2)}, u32[]{:S(2)}) collective-permute-start(bf16[512,128]{1,0:T(8,128)(2,1)S(1)} %constant_dynamic-update-slice_fusion.refs_0_), channel_id=1, source_target_pairs={{0,4},{4,0},{8,12},{12,8},{1,5},{5,1},{9,13},{13,9},{2,6},{6,2},{1... | collective-permute-start | bytes 393224 | tf_op jit(solution)/shard_map/ppermute | solution.py:50
  45.3 6.4 %collective-permute-start.2 = (bf16[512,128]{1,0:T(8,128)(2,1)S(1)}, bf16[512,128]{1,0:T(8,128)(2,1)S(1)}, u32[]{:S(2)}, u32[]{:S(2)}) collective-permute-start(bf16[512,128]{1,0:T(8,128)(2,1)S(1)} %constant_dynamic-update-slice_fusion.refs_0_), channel_id=1, source_target_pairs={{0,8},{4,12},{8,0},{12,4},{1,9},{5,13},{9,1},{13,5},{2,10},{6,14},... | collective-permute-start | bytes 393224 | tf_op jit(solution)/shard_map/ppermute | solution.py:50
  46.8 6.7 %collective-permute-start.3 = (bf16[512,128]{1,0:T(8,128)(2,1)S(1)}, bf16[512,128]{1,0:T(8,128)(2,1)S(1)}, u32[]{:S(2)}, u32[]{:S(2)}) collective-permute-start(bf16[512,128]{1,0:T(8,128)(2,1)S(1)} %constant_dynamic-update-slice_fusion.refs_0_), channel_id=1, source_target_pairs={{0,12},{4,8},{8,4},{12,0},{1,13},{5,9},{9,5},{13,1},{2,14},{6,10},... | collective-permute-start | bytes 393224 | tf_op jit(solution)/shard_map/ppermute | solution.py:50
  47.0 22.4 %collective-permute-start.6 = (bf16[128,2048]{1,0:T(8,128)(2,1)S(1)}, bf16[128,2048]{1,0:T(8,128)(2,1)S(1)}, u32[]{:S(2)}, u32[]{:S(2)}) collective-permute-start(bf16[128,2048]{1,0:T(8,128)(2,1)S(1)} %bitcast.25), channel_id=1, source_target_pairs={{0,1},{1,0},{2,3},{3,2},{4,5},{5,4},{6,7},{7,6},{8,9},{9,8},{10,11... | collective-permute-start | bytes 1572872 | tf_op jit(solution)/shard_map/ppermute | solution.py:50
  49.4 0.7 copy-start
  51.6 0.7 copy-start.2
  53.5 0.6 copy-start.4
  54.1 0.9 copy-start.1
  55.0 0.9 copy-start.3
  55.9 0.9 copy-start.5
  56.8 0.9 copy-start.7
  63.8 11.9 %collective-permute-start.4 = (bf16[128,2048]{1,0:T(8,128)(2,1)}, bf16[128,2048]{1,0:T(8,128)(2,1)}, u32[]{:S(2)}, u32[]{:S(2)}) collective-permute-start(bf16[128,2048]{1,0:T(8,128)(2,1)} %get-tuple-element.16), channel_id=1, source_target_pairs={{0,1},{1,0},{2,3},{3,2},{4,5},{5,4},{6,7},{7,6},{8,9},{9,8},{10,11... | collective-permute-start | bytes 1572872 | tf_op jit(solution)/shard_map/ppermute | solution.py:50
  64.7 14.5 %all-to-all-start.3 = ((bf16[8,16,2048]{2,1,0:T(8,128)(2,1)}), bf16[8,16,2048]{2,1,0:T(8,128)(2,1)S(1)}, u32[]{:S(2)}, u32[]{:S(2)}) async-start(bf16[8,16,2048]{2,1,0:T(8,128)(2,1)} %bitcast.19), calls=%async_computation.3 | async-start | bytes 1048576 | tf_op jit(solution)/shard_map/all_to_all | solution.py:56
  75.3 2.5 %collective-permute-start.7 = (bf16[128,2048]{1,0:T(8,128)(2,1)S(1)}, bf16[128,2048]{1,0:T(8,128)(2,1)S(1)}, u32[]{:S(2)}, u32[]{:S(2)}) collective-permute-start(bf16[128,2048]{1,0:T(8,128)(2,1)S(1)} %get-tuple-element.19), channel_id=1, source_target_pairs={{0,1},{1,0},{2,3},{3,2},{4,5},{5,4},{6,7},{7,6},{8,9},{9,8},{10,11... | collective-permute-start | bytes 1572872 | tf_op jit(solution)/shard_map/ppermute | solution.py:50
  77.8 20.1 %copy-start.8 = (f32[128,2048]{1,0:T(8,128)S(1)}, f32[128,2048]{1,0:T(8,128)}, u32[]{:S(2)}) copy-start(f32[128,2048]{1,0:T(8,128)} %convert_add_fusion) | copy-start | bytes 3145732
  79.2 19.4 %all-to-all-start.1 = ((bf16[8,16,2048]{2,1,0:T(8,128)(2,1)}), bf16[8,16,2048]{2,1,0:T(8,128)(2,1)S(1)}, u32[]{:S(2)}, u32[]{:S(2)}) async-start(bf16[8,16,2048]{2,1,0:T(8,128)(2,1)} %bitcast.15), calls=%async_computation.1 | async-start | bytes 1048576 | tf_op jit(solution)/shard_map/all_to_all | solution.py:56
  84.7 13.2 %collective-permute-start.5 = (bf16[64,2048]{1,0:T(8,128)(2,1)S(1)}, bf16[64,2048]{1,0:T(8,128)(2,1)S(1)}, u32[]{:S(2)}, u32[]{:S(2)}) collective-permute-start(bf16[64,2048]{1,0:T(8,128)(2,1)S(1)} %fusion.1), channel_id=1, source_target_pairs={{0,2},{2,0},{1,3},{3,1},{4,6},{6,4},{5,7},{7,5},{8,10},{10,8},{9,1... | collective-permute-start | bytes 786440 | tf_op jit(solution)/shard_map/ppermute | solution.py:50
  87.5 11.9 %collective-permute-start.11 = (bf16[32,2048]{1,0:T(8,128)(2,1)S(1)}, bf16[32,2048]{1,0:T(8,128)(2,1)S(1)}, u32[]{:S(2)}, u32[]{:S(2)}) collective-permute-start(bf16[32,2048]{1,0:T(8,128)(2,1)S(1)} %shard_map.167), channel_id=1, source_target_pairs={{0,16},{16,0},{1,17},{17,1},{2,18},{18,2},{3,19},{19,3},{4,20},{20... | collective-permute-start | bytes 393224 | tf_op jit(solution)/shard_map/ppermute | solution.py:50

commit v2 on v1

--- a/solution.py
+++ b/solution.py
@@ -15,6 +15,7 @@
 LANES = 128
 DIRECT_MAX = 8
 FLOPS_PER_MICRO = 5e8
+GATE_CUT = 512
 
 WHOLE = "whole"
 VMEM = pl.BlockSpec(memory_space=pltpu.VMEM)
@@ -144,23 +145,35 @@
     out_ref[...] = total.astype(out_ref.dtype)
 
 
+def cuts(total, step):
+    return [(i, min(step, total - i)) for i in range(0, total, step)]
+
+
 def expert_body(
     mine_ref, other_ref, gate_hbm, up_hbm, down_hbm, mine_out, other_out, gate, up, down, sems
 ):
+    spans = cuts(gate.shape[1], GATE_CUT)
     copies = [
-        pltpu.make_async_copy(src.at[0], dst, sems.at[i])
-        for i, (src, dst) in enumerate(((gate_hbm, gate), (up_hbm, up), (down_hbm, down)))
+        pltpu.make_async_copy(
+            gate_hbm.at[0, :, pl.ds(at, size)], gate.at[:, pl.ds(at, size)], sems.at[i]
+        )
+        for i, (at, size) in enumerate(spans)
     ]
+    copies.append(pltpu.make_async_copy(up_hbm.at[0], up, sems.at[len(spans)]))
+    copies.append(pltpu.make_async_copy(down_hbm.at[0], down, sems.at[len(spans) + 1]))
     for copy in copies:
         copy.start()
     rows = jnp.concatenate([mine_ref[...], other_ref[...]], axis=0)
     count = mine_ref.shape[0]
-    copies[0].wait()
-    lhs = jnp.dot(rows, gate[...], preferred_element_type=jnp.float32)
-    copies[1].wait()
+    parts = []
+    for copy, (at, size) in zip(copies, spans):
+        copy.wait()
+        parts.append(jnp.dot(rows, gate[:, at : at + size], preferred_element_type=jnp.float32))
+    lhs = jnp.concatenate(parts, axis=1)
+    copies[-2].wait()
     rhs = jnp.dot(rows, up[...], preferred_element_type=jnp.float32)
     hidden = (lhs / (1.0 + jnp.exp(-lhs)) * rhs).astype(jnp.bfloat16)
-    copies[2].wait()
+    copies[-1].wait()
     out = jnp.dot(hidden, down[...], preferred_element_type=jnp.float32).astype(jnp.bfloat16)
     mine_out[...] = out[:count]
     other_out[...] = out[count:]
@@ -184,7 +197,7 @@
             pltpu.VMEM((width, inner), bf16),
             pltpu.VMEM((width, inner), bf16),
             pltpu.VMEM((inner, width), bf16),
-            pltpu.SemaphoreType.DMA((3,)),
+            pltpu.SemaphoreType.DMA((len(cuts(inner, GATE_CUT)) + 2,)),
         ],
         micros=5.0,
         mib=24,
@@ -342,13 +355,16 @@
     far = swap(joined, "f")
     if near <= DIRECT_MAX:
         pair = jnp.concatenate([joined, far], axis=0)
-        kvs = [pair] + [swap(pair, "n", k) for k in range(1, near)]
+        kvs = [pair]
+        for k in [1 << b for b in reversed(range(near.bit_length() - 1))]:
+            held = kvs[0] if len(kvs) == 1 else jnp.concatenate(kvs, axis=0)
+            kvs = [held, swap(held, "n", k)]
         body = functools.partial(attend_body, head=head, key_heads=key_heads, sides=sides)
         half = ((rows // 2, width), jnp.bfloat16)
         return call(
             body,
             [half, half],
-            [SMEM] + [VMEM] * (len(kvs) + 1) + [WHOLE],
+            [SMEM, WHOLE] + [VMEM] * len(kvs) + [WHOLE],
             (core.reshape(1), rot_q, *kvs, out_weight),
             [pltpu.VMEM(rot_q.shape, jnp.bfloat16)],
             micros=5.0,

time: 101 us -> 99 us (0.980)
  blocking collectives: 13.3 us -> 0 us
  starting transfers between devices: 26.5 us -> 35.1 us
  waiting for transfers between devices: 22.6 us -> 28.7 us
  local copies, waits for them, and re-layouts: 6.65 us -> 1.11 us
  Pallas kernels: 26.6 us -> 29 us
    all_to_all x1 -> x0, blocking collectives: 13.3 us -> none  [exchange(): lax.all_to_all(vals, ('n', 'y'), split_axis=0, concat_axis=0, tiled=True)]
    all_to_all x3 -> x4, waiting for transfers between devices: 0.51 us -> 9.27 us  [exchange(): lax.all_to_all(vals, ('n', 'y'), split_axis=0, concat_axis=0, tiled=True)]
    unnamed x19 -> x6, local copies, waits for them, and re-layouts: 5.57 us -> 0.03 us
    ppermute x12 -> x11, starting transfers between devices: 13.8 us -> 18.9 us  [swap(): return lax.ppermute(vals, axis, [(i, i ^ distance) for i in range(size)])]
    all_to_all x3 -> x4, starting transfers between devices: 12.7 us -> 16.2 us  [exchange(): lax.all_to_all(vals, ('n', 'y'), split_axis=0, concat_axis=0, tiled=True)]
    ppermute x12 -> x11, waiting for transfers between devices: 22.1 us -> 19.4 us  [swap(): return lax.ppermute(vals, axis, [(i, i ^ distance) for i in range(size)])]
    pallas_call x10, Pallas kernels: 26.6 us -> 29 us  [call(): pl.pallas_call(body, grid=(1,), out_shape=[jax.ShapeDtypeStruct(s, d) for...]
  transfers between devices with their start and end apart: 15 -> 15, of which waited for: 6 -> 5; matrix products, arithmetic and copies ran while one was open for 4% -> 4% of each run, Pallas kernels for 23% -> 25%
where the time goes in v2:
time: 99 us; the launch traced here: 98.3 us
  starting transfers between devices  35.1 us (35%)
  Pallas kernels  29 us (29%)
  waiting for transfers between devices  28.7 us (29%)
  other arithmetic  3.62 us (4%)
  local copies, waits for them, and re-layouts  1.11 us (1%)
    pallas_call x10, Pallas kernels, call(): pl.pallas_call(body, grid=(1,), out_shape=[jax.ShapeDtypeStruct(s, d) for...  29 us
    ppermute x11, waiting for transfers between devices, swap(): return lax.ppermute(vals, axis, [(i, i ^ distance) for i in range(size)])  19.4 us
    ppermute x11, starting transfers between devices, swap(): return lax.ppermute(vals, axis, [(i, i ^ distance) for i in range(size)])  18.9 us
    all_to_all x4, starting transfers between devices, exchange(): lax.all_to_all(vals, ('n', 'y'), split_axis=0, concat_axis=0, tiled=True)  16.2 us
    all_to_all x4, waiting for transfers between devices, exchange(): lax.all_to_all(vals, ('n', 'y'), split_axis=0, concat_axis=0, tiled=True)  9.27 us
    add x1, other arithmetic, finish_mixer(): pair = kept.astype(jnp.float32) + swap(sent, 'c').astype(jnp.float32)  2.17 us
  transfers between devices with their start and end apart: 15, of which 5 were waited for; matrix products, arithmetic and copies ran while one was open for 4% of the time, Pallas kernels for 25%

profile of v2, /device:TPU:0, one launch (start us, length us, event | category | flops | bytes accessed | tf_op | source)
XLA Modules:
  0.0 98.3 jit_solution(1463112392877240485)
XLA Ops:
  0.6 2.6 %shard_map.158 = (bf16[32,2176]{1,0:T(8,128)(2,1)S(1)}, bf16[128,2048]{1,0:T(8,128)(2,1)}) custom-call(s32[1]{0:T(128)} %bitcast.6.base_ref, bf16[32,2048]{1,0:T(8,128)(2,1)} %tok_ref.1, f32[1,2048]{1,0:T(1,128)} %bitcast.35, s32[2,32]{1,0:T(2,128)} %bitcast.36, f32[2,32]{1,0:T(2,128)} %bitcast.37), custom_call_target="tpu_custom_call" | custom-call | flops 750000000 | tf_op jit(solution)/shard_map/pallas_call | solution.py:35
  3.2 4.1 %collective-permute-start.7 = (bf16[32,2176]{1,0:T(8,128)(2,1)S(1)}, bf16[32,2176]{1,0:T(8,128)(2,1)S(1)}, u32[]{:S(2)}, u32[]{:S(2)}) collective-permute-start(bf16[32,2176]{1,0:T(8,128)(2,1)S(1)} %get-tuple-element.17.meta_ref), channel_id=1, source_target_pairs={{0,16},{16,0},{1,17},{17,1},{2,18},{18,2},{3,19},{19,3},{4,20},{20... | collective-permute-start | bytes 417800 | tf_op jit(solution)/shard_map/ppermute | solution.py:51
  7.3 6.7 %collective-permute-done.7.far_ref.meta_ref = bf16[32,2176]{1,0:T(8,128)(2,1)S(1)} collective-permute-done((bf16[32,2176]{1,0:T(8,128)(2,1)S(1)}, bf16[32,2176]{1,0:T(8,128)(2,1)S(1)}, u32[]{:S(2)}, u32[]{:S(2)}) %collective-permute-start.7) | collective-permute-done | bytes 139296 | tf_op jit(solution)/shard_map/ppermute | solution.py:51
  14.0 1.5 %shard_map.164 = bf16[128,2048]{1,0:T(8,128)(2,1)} custom-call(s32[1]{0:T(128)} %bitcast.6.base_ref, bf16[32,2176]{1,0:T(8,128)(2,1)S(1)} %collective-permute-done.7.far_ref.meta_ref), custom_call_target="tpu_custom_call" | custom-call | flops 500000000 | tf_op jit(solution)/shard_map/pallas_call | solution.py:35
  15.5 3.9 %all-to-all-start.2 = ((bf16[8,16,2048]{2,1,0:T(8,128)(2,1)}), bf16[8,16,2048]{2,1,0:T(8,128)(2,1)S(1)}, u32[]{:S(2)}, u32[]{:S(2)}) async-start(bf16[8,16,2048]{2,1,0:T(8,128)(2,1)} %bitcast.17), calls=%async_computation.2 | async-start | bytes 1048576 | tf_op jit(solution)/shard_map/all_to_all | solution.py:57
  19.4 9.3 %all-to-all-done.2 = bf16[8,16,2048]{2,1,0:T(8,128)(2,1)S(1)} async-done(((bf16[8,16,2048]{2,1,0:T(8,128)(2,1)}), bf16[8,16,2048]{2,1,0:T(8,128)(2,1)S(1)}, u32[]{:S(2)}, u32[]{:S(2)}) %all-to-all-start.2) | async-done | bytes 524320 | tf_op jit(solution)/shard_map/all_to_all | solution.py:57
  28.6 3.5 %all-to-all-start = ((bf16[8,16,2048]{2,1,0:T(8,128)(2,1)}), bf16[8,16,2048]{2,1,0:T(8,128)(2,1)S(1)}, u32[]{:S(2)}, u32[]{:S(2)}) async-start(bf16[8,16,2048]{2,1,0:T(8,128)(2,1)} %bitcast.13), calls=%async_computation | async-start | bytes 1048576 | tf_op jit(solution)/shard_map/all_to_all | solution.py:57
  32.2 2.3 %shard_map.159 = (bf16[256,256]{1,0:T(8,128)(2,1)S(1)}, bf16[256,128]{1,0:T(8,128)(2,1)S(1)}) custom-call(s32[1]{0:T(128)} %bitcast.1.start_ref, bf16[256,256]{1,0:T(8,128)(2,1)} %q_ref.1, bf16[64,256]{1,0:T(8,128)(2,1)} %bitcast.33, bf16[64,256]{1,0:T(8,128)(2,1)} %bitcast.34, f32[1,64]{1,0:T(1,128)} %bitcast.38, f32[1,64]{1,0:T(1,128)} %bitcast.39, ...), custom_call_target="tpu_custom_call" | custom-call | flops 750000000 | tf_op jit(solution)/shard_map/pallas_call | solution.py:35
  34.5 3.4 %collective-permute-start = (bf16[256,128]{1,0:T(8,128)(2,1)S(1)}, bf16[256,128]{1,0:T(8,128)(2,1)S(1)}, u32[]{:S(2)}, u32[]{:S(2)}) collective-permute-start(bf16[256,128]{1,0:T(8,128)(2,1)S(1)} %get-tuple-element.14), channel_id=1, source_target_pairs={{0,16},{16,0},{1,17},{17,1},{2,18},{18,2},{3,19},{19,3},{4,20},{20... | collective-permute-start | bytes 196616 | tf_op jit(solution)/shard_map/ppermute | solution.py:51
  38.0 2.8 %collective-permute-done = bf16[256,128]{1,0:T(8,128)(2,1)S(1)} collective-permute-done((bf16[256,128]{1,0:T(8,128)(2,1)S(1)}, bf16[256,128]{1,0:T(8,128)(2,1)S(1)}, u32[]{:S(2)}, u32[]{:S(2)}) %collective-permute-start) | collective-permute-done | bytes 65568 | tf_op jit(solution)/shard_map/ppermute | solution.py:51
  40.8 3.1 %collective-permute-start.1 = (bf16[512,128]{1,0:T(8,128)(2,1)S(1)}, bf16[512,128]{1,0:T(8,128)(2,1)S(1)}, u32[]{:S(2)}, u32[]{:S(2)}) collective-permute-start(bf16[512,128]{1,0:T(8,128)(2,1)S(1)} %pad_maximum_fusion), channel_id=1, source_target_pairs={{0,8},{4,12},{8,0},{12,4},{1,9},{5,13},{9,1},{13,5},{2,10},{6,14},... | collective-permute-start | bytes 393224 | tf_op jit(solution)/shard_map/ppermute | solution.py:51
  44.0 2.9 %collective-permute-done.1 = bf16[512,128]{1,0:T(8,128)(2,1)S(1)} collective-permute-done((bf16[512,128]{1,0:T(8,128)(2,1)S(1)}, bf16[512,128]{1,0:T(8,128)(2,1)S(1)}, u32[]{:S(2)}, u32[]{:S(2)}) %collective-permute-start.1) | collective-permute-done | bytes 131104 | tf_op jit(solution)/shard_map/ppermute | solution.py:51
  46.9 1.7 %collective-permute-start.2 = (bf16[1024,128]{1,0:T(8,128)(2,1)S(1)}, bf16[1024,128]{1,0:T(8,128)(2,1)S(1)}, u32[]{:S(2)}, u32[]{:S(2)}) collective-permute-start(bf16[1024,128]{1,0:T(8,128)(2,1)S(1)} %constant_dynamic-update-slice_fusion.refs_0_), channel_id=1, source_target_pairs={{0,4},{4,0},{8,12},{12,8},{1,5},{5,1},{9,13},{13,9},{2,6},{6,2},{1... | collective-permute-start | bytes 786440 | tf_op jit(solution)/shard_map/ppermute | solution.py:51
  48.6 6.5 %shard_map.165 = (bf16[128,2048]{1,0:T(8,128)(2,1)S(1)}, bf16[128,2048]{1,0:T(8,128)(2,1)}) custom-call(bf16[128,2048]{1,0:T(8,128)(2,1)S(1)} %bitcast.28, bf16[128,2048]{1,0:T(8,128)(2,1)S(1)} %collective-permute-done.8.other_ref, bf16[1,2048,896]{2,1,0:T(8,128)(2,1)} %gate_hbm.3, bf16[1,2048,896]{2,1,0:T(8,128)(2,1)} %up_hbm.3, bf16[1,896,2048]{2,1,0:T(8,128)(2,1)} %down_hbm.3), custom_call_target="tpu_custom_call" | custom-call | flops 2500000000 | tf_op jit(solution)/shard_map/pallas_call | solution.py:35
  55.2 0.5 collective-permute-start.5
  55.7 5.3 %shard_map.160 = (bf16[128,2048]{1,0:T(8,128)(2,1)S(1)}, bf16[128,2048]{1,0:T(8,128)(2,1)S(1)}) custom-call(s32[1]{0:T(128)} %bitcast.core_ref, bf16[256,256]{1,0:T(8,128)(2,1)} %copy-done, bf16[1024,128]{1,0:T(8,128)(2,1)S(1)} %constant_dynamic-update-slice_fusion.refs_0_, bf16[1024,128]{1,0:T(8,128)(2,1)S(1)} %collective-permute-done.2.refs_1_, ...), custom_call_target="tpu_custom_call" | custom-call | flops 2500000000 | tf_op jit(solution)/shard_map/pallas_call | solution.py:35
  61.0 0.1 collective-permute-start.3
  61.2 2.0 %shard_map.166 = bf16[128,2048]{1,0:T(8,128)(2,1)} custom-call(bf16[128,2048]{1,0:T(8,128)(2,1)S(1)} %get-tuple-element.20.left_ref, bf16[128,2048]{1,0:T(8,128)(2,1)} %collective-permute-done.9.right_ref), custom_call_target="tpu_custom_call" | custom-call | flops 500000000 | tf_op jit(solution)/shard_map/pallas_call | solution.py:35
  63.1 3.9 %all-to-all-start.3 = ((bf16[8,16,2048]{2,1,0:T(8,128)(2,1)}), bf16[8,16,2048]{2,1,0:T(8,128)(2,1)S(1)}, u32[]{:S(2)}, u32[]{:S(2)}) async-start(bf16[8,16,2048]{2,1,0:T(8,128)(2,1)} %bitcast.19), calls=%async_computation.3 | async-start | bytes 1048576 | tf_op jit(solution)/shard_map/all_to_all | solution.py:57
  67.1 6.5 %shard_map.161 = (bf16[128,2048]{1,0:T(8,128)(2,1)S(1)}, bf16[128,2048]{1,0:T(8,128)(2,1)}) custom-call(bf16[128,2048]{1,0:T(8,128)(2,1)S(1)} %bitcast.26, bf16[128,2048]{1,0:T(8,128)(2,1)S(1)} %collective-permute-done.5.other_ref, bf16[1,2048,896]{2,1,0:T(8,128)(2,1)} %gate_hbm.3, bf16[1,2048,896]{2,1,0:T(8,128)(2,1)} %up_hbm.3, bf16[1,896,2048]{2,1,0:T(8,128)(2,1)} %down_hbm.3), custom_call_target="tpu_custom_call" | custom-call | flops 2500000000 | tf_op jit(solution)/shard_map/pallas_call | solution.py:35
  73.6 0.3 collective-permute-start.6
  73.8 2.2 %convert_add_fusion = f32[128,2048]{1,0:T(8,128)} fusion(bf16[128,2048]{1,0:T(8,128)(2,1)} %collective-permute-done.3, bf16[128,2048]{1,0:T(8,128)(2,1)S(1)} %get-tuple-element.15), kind=kLoop, calls=%fused_computation | loop fusion | flops 786432 | bytes 2097152 | tf_op jit(solution)/shard_map/add | solution.py:388
  76.0 0.9 shard_map.162
  76.9 4.9 %all-to-all-start.1 = ((bf16[8,16,2048]{2,1,0:T(8,128)(2,1)}), bf16[8,16,2048]{2,1,0:T(8,128)(2,1)S(1)}, u32[]{:S(2)}, u32[]{:S(2)}) async-start(bf16[8,16,2048]{2,1,0:T(8,128)(2,1)} %bitcast.15), calls=%async_computation.1 | async-start | bytes 1048576 | tf_op jit(solution)/shard_map/all_to_all | solution.py:57
  81.9 1.1 %fusion.1 = bf16[64,2048]{1,0:T(8,128)(2,1)S(1)} fusion(f32[2,64,2048]{2,1,0:T(8,128)} %bitcast.31, s32[]{:T(128)S(6)} %select_n.8), kind=kLoop, calls=%fused_computation.4 | loop fusion | bytes 524292 | tf_op jit(solution)/shard_map/convert_element_type | solution.py:394
  83.0 2.1 %collective-permute-start.4 = (bf16[64,2048]{1,0:T(8,128)(2,1)S(1)}, bf16[64,2048]{1,0:T(8,128)(2,1)S(1)}, u32[]{:S(2)}, u32[]{:S(2)}) collective-permute-start(bf16[64,2048]{1,0:T(8,128)(2,1)S(1)} %fusion.1), channel_id=1, source_target_pairs={{0,2},{2,0},{1,3},{3,1},{4,6},{6,4},{5,7},{7,5},{8,10},{10,8},{9,1... | collective-permute-start | bytes 786440 | tf_op jit(solution)/shard_map/ppermute | solution.py:51
  85.0 0.7 shard_map.167
  85.8 3.4 %collective-permute-start.10 = (bf16[32,2048]{1,0:T(8,128)(2,1)S(1)}, bf16[32,2048]{1,0:T(8,128)(2,1)S(1)}, u32[]{:S(2)}, u32[]{:S(2)}) collective-permute-start(bf16[32,2048]{1,0:T(8,128)(2,1)S(1)} %shard_map.167), channel_id=1, source_target_pairs={{0,16},{16,0},{1,17},{17,1},{2,18},{18,2},{3,19},{19,3},{4,20},{20... | collective-permute-start | bytes 393224 | tf_op jit(solution)/shard_map/ppermute | solution.py:51
  89.2 7.0 %collective-permute-done.4 = bf16[64,2048]{1,0:T(8,128)(2,1)S(1)} collective-permute-done((bf16[64,2048]{1,0:T(8,128)(2,1)S(1)}, bf16[64,2048]{1,0:T(8,128)(2,1)S(1)}, u32[]{:S(2)}, u32[]{:S(2)}) %collective-permute-start.4) | collective-permute-done | bytes 262176 | tf_op jit(solution)/shard_map/ppermute | solution.py:51
  96.2 0.7 fusion
  96.9 0.7 shard_map.163
  97.7 0.7 add_convert_fusion
  (20 shorter events, 0.2 us)
Async XLA Ops:
  3.2 10.7 %collective-permute-start.7 = (bf16[32,2176]{1,0:T(8,128)(2,1)S(1)}, bf16[32,2176]{1,0:T(8,128)(2,1)S(1)}, u32[]{:S(2)}, u32[]{:S(2)}) collective-permute-start(bf16[32,2176]{1,0:T(8,128)(2,1)S(1)} %get-tuple-element.17.meta_ref), channel_id=1, source_target_pairs={{0,16},{16,0},{1,17},{17,1},{2,18},{18,2},{3,19},{19,3},{4,20},{20... | collective-permute-start | bytes 417800 | tf_op jit(solution)/shard_map/ppermute | solution.py:51
  15.5 13.1 %all-to-all-start.2 = ((bf16[8,16,2048]{2,1,0:T(8,128)(2,1)}), bf16[8,16,2048]{2,1,0:T(8,128)(2,1)S(1)}, u32[]{:S(2)}, u32[]{:S(2)}) async-start(bf16[8,16,2048]{2,1,0:T(8,128)(2,1)} %bitcast.17), calls=%async_computation.2 | async-start | bytes 1048576 | tf_op jit(solution)/shard_map/all_to_all | solution.py:57
  28.6 26.6 %all-to-all-start = ((bf16[8,16,2048]{2,1,0:T(8,128)(2,1)}), bf16[8,16,2048]{2,1,0:T(8,128)(2,1)S(1)}, u32[]{:S(2)}, u32[]{:S(2)}) async-start(bf16[8,16,2048]{2,1,0:T(8,128)(2,1)} %bitcast.13), calls=%async_computation | async-start | bytes 1048576 | tf_op jit(solution)/shard_map/all_to_all | solution.py:57
  32.1 16.5 %collective-permute-start.8 = (bf16[128,2048]{1,0:T(8,128)(2,1)S(1)}, bf16[128,2048]{1,0:T(8,128)(2,1)S(1)}, u32[]{:S(2)}, u32[]{:S(2)}) collective-permute-start(bf16[128,2048]{1,0:T(8,128)(2,1)S(1)} %bitcast.27), channel_id=1, source_target_pairs={{0,1},{1,0},{2,3},{3,2},{4,5},{5,4},{6,7},{7,6},{8,9},{9,8},{10,11... | collective-permute-start | bytes 1572872 | tf_op jit(solution)/shard_map/ppermute | solution.py:51
  34.5 6.3 %copy-start = (bf16[256,256]{1,0:T(8,128)(2,1)}, bf16[256,256]{1,0:T(8,128)(2,1)S(1)}, u32[]{:S(2)}) copy-start(bf16[256,256]{1,0:T(8,128)(2,1)S(1)} %get-tuple-element.13.q_ref) | copy-start | bytes 393220
  34.5 6.3 %collective-permute-start = (bf16[256,128]{1,0:T(8,128)(2,1)S(1)}, bf16[256,128]{1,0:T(8,128)(2,1)S(1)}, u32[]{:S(2)}, u32[]{:S(2)}) collective-permute-start(bf16[256,128]{1,0:T(8,128)(2,1)S(1)} %get-tuple-element.14), channel_id=1, source_target_pairs={{0,16},{16,0},{1,17},{17,1},{2,18},{18,2},{3,19},{19,3},{4,20},{20... | collective-permute-start | bytes 196616 | tf_op jit(solution)/shard_map/ppermute | solution.py:51
  40.8 6.1 %collective-permute-start.1 = (bf16[512,128]{1,0:T(8,128)(2,1)S(1)}, bf16[512,128]{1,0:T(8,128)(2,1)S(1)}, u32[]{:S(2)}, u32[]{:S(2)}) collective-permute-start(bf16[512,128]{1,0:T(8,128)(2,1)S(1)} %pad_maximum_fusion), channel_id=1, source_target_pairs={{0,8},{4,12},{8,0},{12,4},{1,9},{5,13},{9,1},{13,5},{2,10},{6,14},... | collective-permute-start | bytes 393224 | tf_op jit(solution)/shard_map/ppermute | solution.py:51
  46.9 8.8 %collective-permute-start.2 = (bf16[1024,128]{1,0:T(8,128)(2,1)S(1)}, bf16[1024,128]{1,0:T(8,128)(2,1)S(1)}, u32[]{:S(2)}, u32[]{:S(2)}) collective-permute-start(bf16[1024,128]{1,0:T(8,128)(2,1)S(1)} %constant_dynamic-update-slice_fusion.refs_0_), channel_id=1, source_target_pairs={{0,4},{4,0},{8,12},{12,8},{1,5},{5,1},{9,13},{13,9},{2,6},{6,2},{1... | collective-permute-start | bytes 786440 | tf_op jit(solution)/shard_map/ppermute | solution.py:51
  55.2 6.0 %collective-permute-start.9 = (bf16[128,2048]{1,0:T(8,128)(2,1)}, bf16[128,2048]{1,0:T(8,128)(2,1)}, u32[]{:S(2)}, u32[]{:S(2)}) collective-permute-start(bf16[128,2048]{1,0:T(8,128)(2,1)} %get-tuple-element.21), channel_id=1, source_target_pairs={{0,1},{1,0},{2,3},{3,2},{4,5},{5,4},{6,7},{7,6},{8,9},{9,8},{10,11... | collective-permute-start | bytes 1572872 | tf_op jit(solution)/shard_map/ppermute | solution.py:51
  55.2 11.8 %collective-permute-start.5 = (bf16[128,2048]{1,0:T(8,128)(2,1)S(1)}, bf16[128,2048]{1,0:T(8,128)(2,1)S(1)}, u32[]{:S(2)}, u32[]{:S(2)}) collective-permute-start(bf16[128,2048]{1,0:T(8,128)(2,1)S(1)} %bitcast.25), channel_id=1, source_target_pairs={{0,1},{1,0},{2,3},{3,2},{4,5},{5,4},{6,7},{7,6},{8,9},{9,8},{10,11... | collective-permute-start | bytes 1572872 | tf_op jit(solution)/shard_map/ppermute | solution.py:51
  61.0 12.8 %collective-permute-start.3 = (bf16[128,2048]{1,0:T(8,128)(2,1)S(1)}, bf16[128,2048]{1,0:T(8,128)(2,1)}, u32[]{:S(2)}, u32[]{:S(2)}) collective-permute-start(bf16[128,2048]{1,0:T(8,128)(2,1)S(1)} %get-tuple-element.16), channel_id=1, source_target_pairs={{0,1},{1,0},{2,3},{3,2},{4,5},{5,4},{6,7},{7,6},{8,9},{9,8},{10,11... | collective-permute-start | bytes 1572872 | tf_op jit(solution)/shard_map/ppermute | solution.py:51
  63.1 13.8 %all-to-all-start.3 = ((bf16[8,16,2048]{2,1,0:T(8,128)(2,1)}), bf16[8,16,2048]{2,1,0:T(8,128)(2,1)S(1)}, u32[]{:S(2)}, u32[]{:S(2)}) async-start(bf16[8,16,2048]{2,1,0:T(8,128)(2,1)} %bitcast.19), calls=%async_computation.3 | async-start | bytes 1048576 | tf_op jit(solution)/shard_map/all_to_all | solution.py:57
  73.6 2.4 %collective-permute-start.6 = (bf16[128,2048]{1,0:T(8,128)(2,1)}, bf16[128,2048]{1,0:T(8,128)(2,1)S(1)}, u32[]{:S(2)}, u32[]{:S(2)}) collective-permute-start(bf16[128,2048]{1,0:T(8,128)(2,1)} %get-tuple-element.19), channel_id=1, source_target_pairs={{0,1},{1,0},{2,3},{3,2},{4,5},{5,4},{6,7},{7,6},{8,9},{9,8},{10,11... | collective-permute-start | bytes 1572872 | tf_op jit(solution)/shard_map/ppermute | solution.py:51
  76.0 20.2 %copy-start.1 = (f32[128,2048]{1,0:T(8,128)S(1)}, f32[128,2048]{1,0:T(8,128)}, u32[]{:S(2)}) copy-start(f32[128,2048]{1,0:T(8,128)} %convert_add_fusion) | copy-start | bytes 3145732
  76.9 20.0 %all-to-all-start.1 = ((bf16[8,16,2048]{2,1,0:T(8,128)(2,1)}), bf16[8,16,2048]{2,1,0:T(8,128)(2,1)S(1)}, u32[]{:S(2)}, u32[]{:S(2)}) async-start(bf16[8,16,2048]{2,1,0:T(8,128)(2,1)} %bitcast.15), calls=%async_computation.1 | async-start | bytes 1048576 | tf_op jit(solution)/shard_map/all_to_all | solution.py:57
  83.0 13.2 %collective-permute-start.4 = (bf16[64,2048]{1,0:T(8,128)(2,1)S(1)}, bf16[64,2048]{1,0:T(8,128)(2,1)S(1)}, u32[]{:S(2)}, u32[]{:S(2)}) collective-permute-start(bf16[64,2048]{1,0:T(8,128)(2,1)S(1)} %fusion.1), channel_id=1, source_target_pairs={{0,2},{2,0},{1,3},{3,1},{4,6},{6,4},{5,7},{7,5},{8,10},{10,8},{9,1... | collective-permute-start | bytes 786440 | tf_op jit(solution)/shard_map/ppermute | solution.py:51
  85.8 11.9 %collective-permute-start.10 = (bf16[32,2048]{1,0:T(8,128)(2,1)S(1)}, bf16[32,2048]{1,0:T(8,128)(2,1)S(1)}, u32[]{:S(2)}, u32[]{:S(2)}) collective-permute-start(bf16[32,2048]{1,0:T(8,128)(2,1)S(1)} %shard_map.167), channel_id=1, source_target_pairs={{0,16},{16,0},{1,17},{17,1},{2,18},{18,2},{3,19},{19,3},{4,20},{20... | collective-permute-start | bytes 393224 | tf_op jit(solution)/shard_map/ppermute | solution.py:51

commit v3 on v2

--- a/solution.py
+++ b/solution.py
@@ -169,10 +169,12 @@
     for copy, (at, size) in zip(copies, spans):
         copy.wait()
         parts.append(jnp.dot(rows, gate[:, at : at + size], preferred_element_type=jnp.float32))
-    lhs = jnp.concatenate(parts, axis=1)
     copies[-2].wait()
-    rhs = jnp.dot(rows, up[...], preferred_element_type=jnp.float32)
-    hidden = (lhs / (1.0 + jnp.exp(-lhs)) * rhs).astype(jnp.bfloat16)
+    acts = []
+    for lhs, (at, size) in zip(parts, spans):
+        rhs = jnp.dot(rows, up[:, at : at + size], preferred_element_type=jnp.float32)
+        acts.append((lhs / (1.0 + jnp.exp(-lhs)) * rhs).astype(jnp.bfloat16))
+    hidden = jnp.concatenate(acts, axis=1)
     copies[-1].wait()
     out = jnp.dot(hidden, down[...], preferred_element_type=jnp.float32).astype(jnp.bfloat16)
     mine_out[...] = out[:count]

time: 99 us -> 99 us (level)
  no operation moved by 1% of the time
where the time goes in v3:
time: 99 us; the launch traced here: 98.3 us
  starting transfers between devices  35.1 us (35%)
  Pallas kernels  29 us (29%)
  waiting for transfers between devices  28.7 us (29%)
  other arithmetic  3.62 us (4%)
  local copies, waits for them, and re-layouts  1.11 us (1%)
    pallas_call x10, Pallas kernels, call(): pl.pallas_call(body, grid=(1,), out_shape=[jax.ShapeDtypeStruct(s, d) for...  29 us
    ppermute x11, waiting for transfers between devices, swap(): return lax.ppermute(vals, axis, [(i, i ^ distance) for i in range(size)])  19.4 us
    ppermute x11, starting transfers between devices, swap(): return lax.ppermute(vals, axis, [(i, i ^ distance) for i in range(size)])  18.9 us
    all_to_all x4, starting transfers between devices, exchange(): lax.all_to_all(vals, ('n', 'y'), split_axis=0, concat_axis=0, tiled=True)  16.2 us
    all_to_all x4, waiting for transfers between devices, exchange(): lax.all_to_all(vals, ('n', 'y'), split_axis=0, concat_axis=0, tiled=True)  9.27 us
    add x1, other arithmetic, finish_mixer(): pair = kept.astype(jnp.float32) + swap(sent, 'c').astype(jnp.float32)  2.17 us
  transfers between devices with their start and end apart: 15, of which 5 were waited for; matrix products, arithmetic and copies ran while one was open for 4% of the time, Pallas kernels for 25%

profile of v3, /device:TPU:0, one launch (start us, length us, event | category | flops | bytes accessed | tf_op | source)
XLA Modules:
  0.0 98.3 jit_solution(1463112392877240485)
XLA Ops:
  0.6 2.6 %shard_map.158 = (bf16[32,2176]{1,0:T(8,128)(2,1)S(1)}, bf16[128,2048]{1,0:T(8,128)(2,1)}) custom-call(s32[1]{0:T(128)} %bitcast.6.base_ref, bf16[32,2048]{1,0:T(8,128)(2,1)} %tok_ref.1, f32[1,2048]{1,0:T(1,128)} %bitcast.35, s32[2,32]{1,0:T(2,128)} %bitcast.36, f32[2,32]{1,0:T(2,128)} %bitcast.37), custom_call_target="tpu_custom_call" | custom-call | flops 750000000 | tf_op jit(solution)/shard_map/pallas_call | solution.py:35
  3.2 4.1 %collective-permute-start.7 = (bf16[32,2176]{1,0:T(8,128)(2,1)S(1)}, bf16[32,2176]{1,0:T(8,128)(2,1)S(1)}, u32[]{:S(2)}, u32[]{:S(2)}) collective-permute-start(bf16[32,2176]{1,0:T(8,128)(2,1)S(1)} %get-tuple-element.17.meta_ref), channel_id=1, source_target_pairs={{0,16},{16,0},{1,17},{17,1},{2,18},{18,2},{3,19},{19,3},{4,20},{20... | collective-permute-start | bytes 417800 | tf_op jit(solution)/shard_map/ppermute | solution.py:51
  7.3 6.7 %collective-permute-done.7.far_ref.meta_ref = bf16[32,2176]{1,0:T(8,128)(2,1)S(1)} collective-permute-done((bf16[32,2176]{1,0:T(8,128)(2,1)S(1)}, bf16[32,2176]{1,0:T(8,128)(2,1)S(1)}, u32[]{:S(2)}, u32[]{:S(2)}) %collective-permute-start.7) | collective-permute-done | bytes 139296 | tf_op jit(solution)/shard_map/ppermute | solution.py:51
  14.0 1.5 %shard_map.164 = bf16[128,2048]{1,0:T(8,128)(2,1)} custom-call(s32[1]{0:T(128)} %bitcast.6.base_ref, bf16[32,2176]{1,0:T(8,128)(2,1)S(1)} %collective-permute-done.7.far_ref.meta_ref), custom_call_target="tpu_custom_call" | custom-call | flops 500000000 | tf_op jit(solution)/shard_map/pallas_call | solution.py:35
  15.5 3.9 %all-to-all-start.2 = ((bf16[8,16,2048]{2,1,0:T(8,128)(2,1)}), bf16[8,16,2048]{2,1,0:T(8,128)(2,1)S(1)}, u32[]{:S(2)}, u32[]{:S(2)}) async-start(bf16[8,16,2048]{2,1,0:T(8,128)(2,1)} %bitcast.17), calls=%async_computation.2 | async-start | bytes 1048576 | tf_op jit(solution)/shard_map/all_to_all | solution.py:57
  19.4 9.3 %all-to-all-done.2 = bf16[8,16,2048]{2,1,0:T(8,128)(2,1)S(1)} async-done(((bf16[8,16,2048]{2,1,0:T(8,128)(2,1)}), bf16[8,16,2048]{2,1,0:T(8,128)(2,1)S(1)}, u32[]{:S(2)}, u32[]{:S(2)}) %all-to-all-start.2) | async-done | bytes 524320 | tf_op jit(solution)/shard_map/all_to_all | solution.py:57
  28.6 3.5 %all-to-all-start = ((bf16[8,16,2048]{2,1,0:T(8,128)(2,1)}), bf16[8,16,2048]{2,1,0:T(8,128)(2,1)S(1)}, u32[]{:S(2)}, u32[]{:S(2)}) async-start(bf16[8,16,2048]{2,1,0:T(8,128)(2,1)} %bitcast.13), calls=%async_computation | async-start | bytes 1048576 | tf_op jit(solution)/shard_map/all_to_all | solution.py:57
  32.2 2.3 %shard_map.159 = (bf16[256,256]{1,0:T(8,128)(2,1)S(1)}, bf16[256,128]{1,0:T(8,128)(2,1)S(1)}) custom-call(s32[1]{0:T(128)} %bitcast.1.start_ref, bf16[256,256]{1,0:T(8,128)(2,1)} %q_ref.1, bf16[64,256]{1,0:T(8,128)(2,1)} %bitcast.33, bf16[64,256]{1,0:T(8,128)(2,1)} %bitcast.34, f32[1,64]{1,0:T(1,128)} %bitcast.38, f32[1,64]{1,0:T(1,128)} %bitcast.39, ...), custom_call_target="tpu_custom_call" | custom-call | flops 750000000 | tf_op jit(solution)/shard_map/pallas_call | solution.py:35
  34.5 3.4 %collective-permute-start = (bf16[256,128]{1,0:T(8,128)(2,1)S(1)}, bf16[256,128]{1,0:T(8,128)(2,1)S(1)}, u32[]{:S(2)}, u32[]{:S(2)}) collective-permute-start(bf16[256,128]{1,0:T(8,128)(2,1)S(1)} %get-tuple-element.14), channel_id=1, source_target_pairs={{0,16},{16,0},{1,17},{17,1},{2,18},{18,2},{3,19},{19,3},{4,20},{20... | collective-permute-start | bytes 196616 | tf_op jit(solution)/shard_map/ppermute | solution.py:51
  38.0 2.8 %collective-permute-done = bf16[256,128]{1,0:T(8,128)(2,1)S(1)} collective-permute-done((bf16[256,128]{1,0:T(8,128)(2,1)S(1)}, bf16[256,128]{1,0:T(8,128)(2,1)S(1)}, u32[]{:S(2)}, u32[]{:S(2)}) %collective-permute-start) | collective-permute-done | bytes 65568 | tf_op jit(solution)/shard_map/ppermute | solution.py:51
  40.8 3.1 %collective-permute-start.1 = (bf16[512,128]{1,0:T(8,128)(2,1)S(1)}, bf16[512,128]{1,0:T(8,128)(2,1)S(1)}, u32[]{:S(2)}, u32[]{:S(2)}) collective-permute-start(bf16[512,128]{1,0:T(8,128)(2,1)S(1)} %pad_maximum_fusion), channel_id=1, source_target_pairs={{0,8},{4,12},{8,0},{12,4},{1,9},{5,13},{9,1},{13,5},{2,10},{6,14},... | collective-permute-start | bytes 393224 | tf_op jit(solution)/shard_map/ppermute | solution.py:51
  44.0 2.9 %collective-permute-done.1 = bf16[512,128]{1,0:T(8,128)(2,1)S(1)} collective-permute-done((bf16[512,128]{1,0:T(8,128)(2,1)S(1)}, bf16[512,128]{1,0:T(8,128)(2,1)S(1)}, u32[]{:S(2)}, u32[]{:S(2)}) %collective-permute-start.1) | collective-permute-done | bytes 131104 | tf_op jit(solution)/shard_map/ppermute | solution.py:51
  46.9 1.7 %collective-permute-start.2 = (bf16[1024,128]{1,0:T(8,128)(2,1)S(1)}, bf16[1024,128]{1,0:T(8,128)(2,1)S(1)}, u32[]{:S(2)}, u32[]{:S(2)}) collective-permute-start(bf16[1024,128]{1,0:T(8,128)(2,1)S(1)} %constant_dynamic-update-slice_fusion.refs_0_), channel_id=1, source_target_pairs={{0,4},{4,0},{8,12},{12,8},{1,5},{5,1},{9,13},{13,9},{2,6},{6,2},{1... | collective-permute-start | bytes 786440 | tf_op jit(solution)/shard_map/ppermute | solution.py:51
  48.6 6.5 %shard_map.165 = (bf16[128,2048]{1,0:T(8,128)(2,1)S(1)}, bf16[128,2048]{1,0:T(8,128)(2,1)}) custom-call(bf16[128,2048]{1,0:T(8,128)(2,1)S(1)} %bitcast.28, bf16[128,2048]{1,0:T(8,128)(2,1)S(1)} %collective-permute-done.8.other_ref, bf16[1,2048,896]{2,1,0:T(8,128)(2,1)} %gate_hbm.3, bf16[1,2048,896]{2,1,0:T(8,128)(2,1)} %up_hbm.3, bf16[1,896,2048]{2,1,0:T(8,128)(2,1)} %down_hbm.3), custom_call_target="tpu_custom_call" | custom-call | flops 2500000000 | tf_op jit(solution)/shard_map/pallas_call | solution.py:35
  55.2 0.5 collective-permute-start.5
  55.7 5.3 %shard_map.160 = (bf16[128,2048]{1,0:T(8,128)(2,1)S(1)}, bf16[128,2048]{1,0:T(8,128)(2,1)S(1)}) custom-call(s32[1]{0:T(128)} %bitcast.core_ref, bf16[256,256]{1,0:T(8,128)(2,1)} %copy-done, bf16[1024,128]{1,0:T(8,128)(2,1)S(1)} %constant_dynamic-update-slice_fusion.refs_0_, bf16[1024,128]{1,0:T(8,128)(2,1)S(1)} %collective-permute-done.2.refs_1_, ...), custom_call_target="tpu_custom_call" | custom-call | flops 2500000000 | tf_op jit(solution)/shard_map/pallas_call | solution.py:35
  61.0 0.1 collective-permute-start.3
  61.2 2.0 %shard_map.166 = bf16[128,2048]{1,0:T(8,128)(2,1)} custom-call(bf16[128,2048]{1,0:T(8,128)(2,1)S(1)} %get-tuple-element.20.left_ref, bf16[128,2048]{1,0:T(8,128)(2,1)} %collective-permute-done.9.right_ref), custom_call_target="tpu_custom_call" | custom-call | flops 500000000 | tf_op jit(solution)/shard_map/pallas_call | solution.py:35
  63.1 3.9 %all-to-all-start.3 = ((bf16[8,16,2048]{2,1,0:T(8,128)(2,1)}), bf16[8,16,2048]{2,1,0:T(8,128)(2,1)S(1)}, u32[]{:S(2)}, u32[]{:S(2)}) async-start(bf16[8,16,2048]{2,1,0:T(8,128)(2,1)} %bitcast.19), calls=%async_computation.3 | async-start | bytes 1048576 | tf_op jit(solution)/shard_map/all_to_all | solution.py:57
  67.1 6.5 %shard_map.161 = (bf16[128,2048]{1,0:T(8,128)(2,1)S(1)}, bf16[128,2048]{1,0:T(8,128)(2,1)}) custom-call(bf16[128,2048]{1,0:T(8,128)(2,1)S(1)} %bitcast.26, bf16[128,2048]{1,0:T(8,128)(2,1)S(1)} %collective-permute-done.5.other_ref, bf16[1,2048,896]{2,1,0:T(8,128)(2,1)} %gate_hbm.3, bf16[1,2048,896]{2,1,0:T(8,128)(2,1)} %up_hbm.3, bf16[1,896,2048]{2,1,0:T(8,128)(2,1)} %down_hbm.3), custom_call_target="tpu_custom_call" | custom-call | flops 2500000000 | tf_op jit(solution)/shard_map/pallas_call | solution.py:35
  73.6 0.3 collective-permute-start.6
  73.8 2.2 %convert_add_fusion = f32[128,2048]{1,0:T(8,128)} fusion(bf16[128,2048]{1,0:T(8,128)(2,1)} %collective-permute-done.3, bf16[128,2048]{1,0:T(8,128)(2,1)S(1)} %get-tuple-element.15), kind=kLoop, calls=%fused_computation | loop fusion | flops 786432 | bytes 2097152 | tf_op jit(solution)/shard_map/add | solution.py:390
  76.0 0.9 shard_map.162
  76.9 4.9 %all-to-all-start.1 = ((bf16[8,16,2048]{2,1,0:T(8,128)(2,1)}), bf16[8,16,2048]{2,1,0:T(8,128)(2,1)S(1)}, u32[]{:S(2)}, u32[]{:S(2)}) async-start(bf16[8,16,2048]{2,1,0:T(8,128)(2,1)} %bitcast.15), calls=%async_computation.1 | async-start | bytes 1048576 | tf_op jit(solution)/shard_map/all_to_all | solution.py:57
  81.9 1.1 %fusion.1 = bf16[64,2048]{1,0:T(8,128)(2,1)S(1)} fusion(f32[2,64,2048]{2,1,0:T(8,128)} %bitcast.31, s32[]{:T(128)S(6)} %select_n.8), kind=kLoop, calls=%fused_computation.4 | loop fusion | bytes 524292 | tf_op jit(solution)/shard_map/convert_element_type | solution.py:396
  83.0 2.1 %collective-permute-start.4 = (bf16[64,2048]{1,0:T(8,128)(2,1)S(1)}, bf16[64,2048]{1,0:T(8,128)(2,1)S(1)}, u32[]{:S(2)}, u32[]{:S(2)}) collective-permute-start(bf16[64,2048]{1,0:T(8,128)(2,1)S(1)} %fusion.1), channel_id=1, source_target_pairs={{0,2},{2,0},{1,3},{3,1},{4,6},{6,4},{5,7},{7,5},{8,10},{10,8},{9,1... | collective-permute-start | bytes 786440 | tf_op jit(solution)/shard_map/ppermute | solution.py:51
  85.0 0.7 shard_map.167
  85.8 3.4 %collective-permute-start.10 = (bf16[32,2048]{1,0:T(8,128)(2,1)S(1)}, bf16[32,2048]{1,0:T(8,128)(2,1)S(1)}, u32[]{:S(2)}, u32[]{:S(2)}) collective-permute-start(bf16[32,2048]{1,0:T(8,128)(2,1)S(1)} %shard_map.167), channel_id=1, source_target_pairs={{0,16},{16,0},{1,17},{17,1},{2,18},{18,2},{3,19},{19,3},{4,20},{20... | collective-permute-start | bytes 393224 | tf_op jit(solution)/shard_map/ppermute | solution.py:51
  89.2 7.0 %collective-permute-done.4 = bf16[64,2048]{1,0:T(8,128)(2,1)S(1)} collective-permute-done((bf16[64,2048]{1,0:T(8,128)(2,1)S(1)}, bf16[64,2048]{1,0:T(8,128)(2,1)S(1)}, u32[]{:S(2)}, u32[]{:S(2)}) %collective-permute-start.4) | collective-permute-done | bytes 262176 | tf_op jit(solution)/shard_map/ppermute | solution.py:51
  96.2 0.7 fusion
  96.9 0.7 shard_map.163
  97.7 0.7 add_convert_fusion
  (20 shorter events, 0.2 us)
Async XLA Ops:
  3.2 10.7 %collective-permute-start.7 = (bf16[32,2176]{1,0:T(8,128)(2,1)S(1)}, bf16[32,2176]{1,0:T(8,128)(2,1)S(1)}, u32[]{:S(2)}, u32[]{:S(2)}) collective-permute-start(bf16[32,2176]{1,0:T(8,128)(2,1)S(1)} %get-tuple-element.17.meta_ref), channel_id=1, source_target_pairs={{0,16},{16,0},{1,17},{17,1},{2,18},{18,2},{3,19},{19,3},{4,20},{20... | collective-permute-start | bytes 417800 | tf_op jit(solution)/shard_map/ppermute | solution.py:51
  15.5 13.1 %all-to-all-start.2 = ((bf16[8,16,2048]{2,1,0:T(8,128)(2,1)}), bf16[8,16,2048]{2,1,0:T(8,128)(2,1)S(1)}, u32[]{:S(2)}, u32[]{:S(2)}) async-start(bf16[8,16,2048]{2,1,0:T(8,128)(2,1)} %bitcast.17), calls=%async_computation.2 | async-start | bytes 1048576 | tf_op jit(solution)/shard_map/all_to_all | solution.py:57
  28.6 26.6 %all-to-all-start = ((bf16[8,16,2048]{2,1,0:T(8,128)(2,1)}), bf16[8,16,2048]{2,1,0:T(8,128)(2,1)S(1)}, u32[]{:S(2)}, u32[]{:S(2)}) async-start(bf16[8,16,2048]{2,1,0:T(8,128)(2,1)} %bitcast.13), calls=%async_computation | async-start | bytes 1048576 | tf_op jit(solution)/shard_map/all_to_all | solution.py:57
  32.1 16.5 %collective-permute-start.8 = (bf16[128,2048]{1,0:T(8,128)(2,1)S(1)}, bf16[128,2048]{1,0:T(8,128)(2,1)S(1)}, u32[]{:S(2)}, u32[]{:S(2)}) collective-permute-start(bf16[128,2048]{1,0:T(8,128)(2,1)S(1)} %bitcast.27), channel_id=1, source_target_pairs={{0,1},{1,0},{2,3},{3,2},{4,5},{5,4},{6,7},{7,6},{8,9},{9,8},{10,11... | collective-permute-start | bytes 1572872 | tf_op jit(solution)/shard_map/ppermute | solution.py:51
  34.5 6.3 %copy-start = (bf16[256,256]{1,0:T(8,128)(2,1)}, bf16[256,256]{1,0:T(8,128)(2,1)S(1)}, u32[]{:S(2)}) copy-start(bf16[256,256]{1,0:T(8,128)(2,1)S(1)} %get-tuple-element.13.q_ref) | copy-start | bytes 393220
  34.5 6.3 %collective-permute-start = (bf16[256,128]{1,0:T(8,128)(2,1)S(1)}, bf16[256,128]{1,0:T(8,128)(2,1)S(1)}, u32[]{:S(2)}, u32[]{:S(2)}) collective-permute-start(bf16[256,128]{1,0:T(8,128)(2,1)S(1)} %get-tuple-element.14), channel_id=1, source_target_pairs={{0,16},{16,0},{1,17},{17,1},{2,18},{18,2},{3,19},{19,3},{4,20},{20... | collective-permute-start | bytes 196616 | tf_op jit(solution)/shard_map/ppermute | solution.py:51
  40.8 6.1 %collective-permute-start.1 = (bf16[512,128]{1,0:T(8,128)(2,1)S(1)}, bf16[512,128]{1,0:T(8,128)(2,1)S(1)}, u32[]{:S(2)}, u32[]{:S(2)}) collective-permute-start(bf16[512,128]{1,0:T(8,128)(2,1)S(1)} %pad_maximum_fusion), channel_id=1, source_target_pairs={{0,8},{4,12},{8,0},{12,4},{1,9},{5,13},{9,1},{13,5},{2,10},{6,14},... | collective-permute-start | bytes 393224 | tf_op jit(solution)/shard_map/ppermute | solution.py:51
  46.9 8.8 %collective-permute-start.2 = (bf16[1024,128]{1,0:T(8,128)(2,1)S(1)}, bf16[1024,128]{1,0:T(8,128)(2,1)S(1)}, u32[]{:S(2)}, u32[]{:S(2)}) collective-permute-start(bf16[1024,128]{1,0:T(8,128)(2,1)S(1)} %constant_dynamic-update-slice_fusion.refs_0_), channel_id=1, source_target_pairs={{0,4},{4,0},{8,12},{12,8},{1,5},{5,1},{9,13},{13,9},{2,6},{6,2},{1... | collective-permute-start | bytes 786440 | tf_op jit(solution)/shard_map/ppermute | solution.py:51
  55.2 6.0 %collective-permute-start.9 = (bf16[128,2048]{1,0:T(8,128)(2,1)}, bf16[128,2048]{1,0:T(8,128)(2,1)}, u32[]{:S(2)}, u32[]{:S(2)}) collective-permute-start(bf16[128,2048]{1,0:T(8,128)(2,1)} %get-tuple-element.21), channel_id=1, source_target_pairs={{0,1},{1,0},{2,3},{3,2},{4,5},{5,4},{6,7},{7,6},{8,9},{9,8},{10,11... | collective-permute-start | bytes 1572872 | tf_op jit(solution)/shard_map/ppermute | solution.py:51
  55.2 11.8 %collective-permute-start.5 = (bf16[128,2048]{1,0:T(8,128)(2,1)S(1)}, bf16[128,2048]{1,0:T(8,128)(2,1)S(1)}, u32[]{:S(2)}, u32[]{:S(2)}) collective-permute-start(bf16[128,2048]{1,0:T(8,128)(2,1)S(1)} %bitcast.25), channel_id=1, source_target_pairs={{0,1},{1,0},{2,3},{3,2},{4,5},{5,4},{6,7},{7,6},{8,9},{9,8},{10,11... | collective-permute-start | bytes 1572872 | tf_op jit(solution)/shard_map/ppermute | solution.py:51
  61.0 12.8 %collective-permute-start.3 = (bf16[128,2048]{1,0:T(8,128)(2,1)S(1)}, bf16[128,2048]{1,0:T(8,128)(2,1)}, u32[]{:S(2)}, u32[]{:S(2)}) collective-permute-start(bf16[128,2048]{1,0:T(8,128)(2,1)S(1)} %get-tuple-element.16), channel_id=1, source_target_pairs={{0,1},{1,0},{2,3},{3,2},{4,5},{5,4},{6,7},{7,6},{8,9},{9,8},{10,11... | collective-permute-start | bytes 1572872 | tf_op jit(solution)/shard_map/ppermute | solution.py:51
  63.1 13.8 %all-to-all-start.3 = ((bf16[8,16,2048]{2,1,0:T(8,128)(2,1)}), bf16[8,16,2048]{2,1,0:T(8,128)(2,1)S(1)}, u32[]{:S(2)}, u32[]{:S(2)}) async-start(bf16[8,16,2048]{2,1,0:T(8,128)(2,1)} %bitcast.19), calls=%async_computation.3 | async-start | bytes 1048576 | tf_op jit(solution)/shard_map/all_to_all | solution.py:57
  73.6 2.4 %collective-permute-start.6 = (bf16[128,2048]{1,0:T(8,128)(2,1)}, bf16[128,2048]{1,0:T(8,128)(2,1)S(1)}, u32[]{:S(2)}, u32[]{:S(2)}) collective-permute-start(bf16[128,2048]{1,0:T(8,128)(2,1)} %get-tuple-element.19), channel_id=1, source_target_pairs={{0,1},{1,0},{2,3},{3,2},{4,5},{5,4},{6,7},{7,6},{8,9},{9,8},{10,11... | collective-permute-start | bytes 1572872 | tf_op jit(solution)/shard_map/ppermute | solution.py:51
  76.0 20.2 %copy-start.1 = (f32[128,2048]{1,0:T(8,128)S(1)}, f32[128,2048]{1,0:T(8,128)}, u32[]{:S(2)}) copy-start(f32[128,2048]{1,0:T(8,128)} %convert_add_fusion) | copy-start | bytes 3145732
  76.9 20.0 %all-to-all-start.1 = ((bf16[8,16,2048]{2,1,0:T(8,128)(2,1)}), bf16[8,16,2048]{2,1,0:T(8,128)(2,1)S(1)}, u32[]{:S(2)}, u32[]{:S(2)}) async-start(bf16[8,16,2048]{2,1,0:T(8,128)(2,1)} %bitcast.15), calls=%async_computation.1 | async-start | bytes 1048576 | tf_op jit(solution)/shard_map/all_to_all | solution.py:57
  83.0 13.2 %collective-permute-start.4 = (bf16[64,2048]{1,0:T(8,128)(2,1)S(1)}, bf16[64,2048]{1,0:T(8,128)(2,1)S(1)}, u32[]{:S(2)}, u32[]{:S(2)}) collective-permute-start(bf16[64,2048]{1,0:T(8,128)(2,1)S(1)} %fusion.1), channel_id=1, source_target_pairs={{0,2},{2,0},{1,3},{3,1},{4,6},{6,4},{5,7},{7,5},{8,10},{10,8},{9,1... | collective-permute-start | bytes 786440 | tf_op jit(solution)/shard_map/ppermute | solution.py:51
  85.8 11.9 %collective-permute-start.10 = (bf16[32,2048]{1,0:T(8,128)(2,1)S(1)}, bf16[32,2048]{1,0:T(8,128)(2,1)S(1)}, u32[]{:S(2)}, u32[]{:S(2)}) collective-permute-start(bf16[32,2048]{1,0:T(8,128)(2,1)S(1)} %shard_map.167), channel_id=1, source_target_pairs={{0,16},{16,0},{1,17},{17,1},{2,18},{18,2},{3,19},{19,3},{4,20},{20... | collective-permute-start | bytes 393224 | tf_op jit(solution)/shard_map/ppermute | solution.py:51
